TPU v7x, 256 devices: a 4x2x16 block of a 4x16x16 slice. The times are simulated.
256 devices in a mesh: grp: 2 (over y), sp: 16 (over z), fs: 4 (over x), tp: 2 (over core).
Axes of the slice: x: 4, y: 2, z: 16, core: 2. Of those that a mesh axis runs over, the one named last changes fastest.
The devices are a block of a 4x16x16 slice.
Arguments:
- tokens: bfloat16 [16, 2048, 2048], P(('grp', 'fs'), ('sp', 'tp')), parts along dimension 0, may hold values from -24 to 24
- norm_gain: float32 [2048], replicated, may hold values from 0.1 to 1.9
- w_query: bfloat16 [2048, 1024], P(('sp', 'fs'), 'tp'), may hold values from -0.125 to 0.125
- w_key: bfloat16 [2048, 1024], P(('sp', 'fs'), 'tp'), may hold values from -0.125 to 0.125
- w_value: bfloat16 [2048, 1024], P(('sp', 'fs'), 'tp'), may hold values from -0.125 to 0.125
- query_gain: float32 [1024], P('tp'), may hold values from 1 to 26
- key_gain: float32 [1024], P('tp'), may hold values from 0.1 to 1.9
- mix_lambda: float32 [8], P('tp'), may hold values from 0.3 to 0.8
- head_gain: float32 [128], replicated, may hold values from 0.1 to 1.9
- w_gate_b: bfloat16 [2048, 1024], P(('sp', 'fs'), 'tp'), may hold values from -0.125 to 0.125
- w_gate_c: bfloat16 [2048, 1024], P(('sp', 'fs'), 'tp'), may hold values from -0.125 to 0.125
- w_conv_in: bfloat16 [2048, 1024], P(('sp', 'fs'), 'tp'), may hold values from -0.125 to 0.125
- conv_taps: float32 [3, 1024], P(None, 'tp'), may hold values from -3 to 3
- w_out_attn: bfloat16 [1024, 2048], P('tp', ('sp', 'fs')), may hold values from -0.125 to 0.125
- w_out_conv: bfloat16 [1024, 2048], P('tp', ('sp', 'fs')), may hold values from -0.125 to 0.125
Outputs:
- mixed: bfloat16 [16, 2048, 2048], P(('grp', 'fs'), ('sp', 'tp')), parts along dimension 0
There are 2 independent parts, one for each index of `grp`. A program takes and returns all parts, laid end to end along the dimension named above; an argument that names none is the same for every part. Nothing has to cross between parts.
All inputs are finite; a program needn't handle non-finite values.
Results may differ from a plain program's by a relative error of at most 0.04.
Values may be sent and summed in bfloat16 or wider, within the bound.
A program may use at most 128 MiB of HBM per device.

v0:
```python
import math

import jax
import jax.numpy as jnp
from jax import lax
from jax.sharding import PartitionSpec as P

DK = 64
DV = 128
KW = 3


EPS = 1e-06
NEG = -1e30
OUT_SCALE = 0.8


def in_one_piece(arrays, axis, dim, along):
    ends, at = ([], 0)
    for a in arrays[:-1]:
        at += a.shape[along]
        ends.append(at)
    both = jnp.concatenate(arrays, axis=along)
    return tuple(jnp.split(lax.all_gather(both, axis, axis=dim, tiled=True), ends, axis=along))


def from_behind(block, axis, distance):
    devices = range(lax.axis_size(axis))
    route = [(i - distance, i) for i in devices if i - distance in devices]
    return lax.ppermute(block, axis, route)


def copy_for_each(value, axis):
    copies = jnp.broadcast_to(value, (lax.axis_size(axis), *value.shape))
    return lax.all_to_all(copies, axis, split_axis=0, concat_axis=0, tiled=True)


def joined_along(tiles, dim):
    lengths = list(tiles.shape[1:])
    lengths[dim] *= tiles.shape[0]
    return jnp.moveaxis(tiles, 0, dim).reshape(lengths)


def gather_directly(value, axis, dim):
    tiles = copy_for_each(value, axis)
    return joined_along(tiles, dim)


def turned_gather(arrays, axis, dims):
    turned = [jnp.moveaxis(a, dim, 0) for a, dim in zip(arrays, dims)]
    both = jnp.concatenate([t.reshape(len(t), -1) for t in turned], axis=1)
    whole, at, finished = (lax.all_gather(both, axis, axis=0, tiled=True), 0, [])
    for t, dim in zip(turned, dims):
        piece = whole[:, at : at + t[0].size].reshape(-1, *t.shape[1:])
        finished.append(jnp.moveaxis(piece, 0, dim))
        at += t[0].size
    return tuple(finished)


def in_blocks(value, dim, count):
    lengths = value.shape
    tiles = value.reshape(*lengths[:dim], count, lengths[dim] // count, *lengths[dim + 1 :])
    return jnp.moveaxis(tiles, dim, 0)


def sent_and_summed(value, axis, dim):
    tiles = in_blocks(value, dim, lax.axis_size(axis))
    arrived = lax.all_to_all(tiles, axis, split_axis=0, concat_axis=0, tiled=True)
    return arrived.astype(jnp.float32).sum(axis=0)


def rms_scale(values, gain):
    wide = values.astype(jnp.float32)
    return wide * lax.rsqrt(jnp.mean(wide * wide, axis=-1, keepdims=True) + EPS) * gain


def attend_heads(normed, wq_full, wk_full, wv_full, query_gain, key_gain, mix_lambda, head_gain):
    rows = normed.shape[0]
    heads_here = mix_lambda.shape[0]
    query = rms_scale(
        jnp.dot(normed, wq_full, preferred_element_type=jnp.float32)
        .astype(jnp.bfloat16)
        .reshape(rows, heads_here, 2, DK),
        query_gain.reshape(heads_here, 2, DK),
    ).astype(jnp.bfloat16)
    key = rms_scale(
        jnp.dot(normed, wk_full, preferred_element_type=jnp.float32)
        .astype(jnp.bfloat16)
        .reshape(rows, heads_here, 2, DK),
        key_gain.reshape(heads_here, 2, DK),
    ).astype(jnp.bfloat16)
    value = jnp.dot(normed, wv_full, preferred_element_type=jnp.float32).astype(jnp.bfloat16)
    q_pos = lax.axis_index("sp") * rows + jnp.arange(rows, dtype=jnp.int32)
    init = (
        jnp.full((heads_here, 2, rows), NEG, jnp.float32),
        jnp.zeros((heads_here, 2, rows), jnp.float32),
        jnp.zeros((heads_here, 2, rows, DV), jnp.float32),
    )
    key_piece, value_piece = in_one_piece(
        (key.reshape(rows, heads_here * 2 * DK), value), "sp", 0, 1
    )
    count = key_piece.shape[0]
    width = math.gcd(count, 1024)
    blocks = count // width
    key_blocks = key_piece.reshape(blocks, width, heads_here, 2, DK)
    value_blocks = value_piece.reshape(blocks, width, heads_here, DV)
    begins = jnp.arange(blocks, dtype=jnp.int32) * width

    def step(state, inputs):
        running, total, summed = state
        key_block, value_block, begin = inputs
        k_pos = begin + jnp.arange(width, dtype=jnp.int32)
        score = jnp.einsum(
            "qhmd,khmd->hmqk", query, key_block, preferred_element_type=jnp.float32
        ) * DK ** (-0.5)
        allowed = k_pos[None, :] <= q_pos[:, None]
        score = jnp.where(allowed, score, NEG)
        newest = jnp.maximum(running, jnp.max(score, axis=-1))
        factor = jnp.exp(running - newest)
        weights = jnp.where(allowed, jnp.exp(score - newest[..., None]), 0.0)
        total = total * factor + jnp.sum(weights, axis=-1)
        summed = summed * factor[..., None] + jnp.einsum(
            "hmqk,khd->hmqd",
            weights.astype(jnp.bfloat16),
            value_block,
            preferred_element_type=jnp.float32,
        )
        return ((newest, total, summed), None)

    result, unused = lax.scan(step, init, (key_blocks, value_blocks, begins))
    running, total, summed = result
    head_map = summed / total[..., None]
    differ = head_map[:, 0] - mix_lambda[:, None, None] * head_map[:, 1]
    normal = rms_scale(differ, head_gain) * OUT_SCALE
    return normal.transpose(1, 0, 2).reshape(rows, heads_here * DV).astype(jnp.bfloat16)


def gated_conv(normed, wb_full, wc_full, wi_full, conv_taps):
    rows = normed.shape[0]
    gate_b = jnp.dot(normed, wb_full, preferred_element_type=jnp.float32).astype(jnp.bfloat16)
    gate_c = jnp.dot(normed, wc_full, preferred_element_type=jnp.float32).astype(jnp.bfloat16)
    conv_in = jnp.dot(normed, wi_full, preferred_element_type=jnp.float32).astype(jnp.bfloat16)
    shaped = (gate_c.astype(jnp.float32) * conv_in.astype(jnp.float32)).astype(jnp.bfloat16)
    edge = from_behind(shaped[rows - (KW - 1) :], "sp", 1)
    padded = jnp.concatenate([edge, shaped], axis=0).astype(jnp.float32)
    conv = conv_taps[0][None, :] * padded[0:rows]
    for tap in range(1, KW):
        conv = conv + conv_taps[tap][None, :] * padded[tap : tap + rows]
    return (gate_b.astype(jnp.float32) * conv).astype(jnp.bfloat16)


def normalize_rows(own_rows, norm_gain):
    return rms_scale(gather_directly(own_rows, "tp", 0), norm_gain).astype(jnp.bfloat16)


def on_device(
    tokens,
    norm_gain,
    w_query,
    w_key,
    w_value,
    query_gain,
    key_gain,
    mix_lambda,
    head_gain,
    w_gate_b,
    w_gate_c,
    w_conv_in,
    conv_taps,
    w_out_attn,
    w_out_conv,
):
    seq_count = tokens.shape[0]
    gathered = turned_gather(
        (w_query, w_key, w_value, w_gate_b, w_gate_c, w_conv_in, w_out_attn, w_out_conv),
        ("sp", "fs"),
        (0, 0, 0, 0, 0, 0, 1, 1),
    )
    normed_list = [normalize_rows(tokens[index], norm_gain) for index in range(seq_count)]
    attn_list = [
        attend_heads(
            normed,
            gathered[0],
            gathered[1],
            gathered[2],
            query_gain,
            key_gain,
            mix_lambda,
            head_gain,
        )
        for normed in normed_list
    ]
    conv_list = [
        gated_conv(normed, gathered[3], gathered[4], gathered[5], conv_taps)
        for normed in normed_list
    ]
    out_attn = gathered[6]
    out_conv = gathered[7]
    results = []
    for index in range(seq_count):
        attn = attn_list[index]
        conv_out = conv_list[index]
        results.append(
            sent_and_summed(
                (
                    jnp.dot(attn, out_attn, preferred_element_type=jnp.float32)
                    + jnp.dot(conv_out, out_conv, preferred_element_type=jnp.float32)
                ).astype(jnp.bfloat16),
                "tp",
                0,
            ).astype(jnp.bfloat16)
        )
    return jnp.stack(results, axis=0)


def solution(mesh):
    placed = (
        P(("grp", "fs"), ("sp", "tp"), None),
        P(),
        P(("sp", "fs"), "tp"),
        P(("sp", "fs"), "tp"),
        P(("sp", "fs"), "tp"),
        P("tp"),
        P("tp"),
        P("tp"),
        P(),
        P(("sp", "fs"), "tp"),
        P(("sp", "fs"), "tp"),
        P(("sp", "fs"), "tp"),
        P(None, "tp"),
        P("tp", ("sp", "fs")),
        P("tp", ("sp", "fs")),
    )
    return jax.shard_map(
        on_device,
        mesh=mesh,
        in_specs=placed,
        out_specs=P(("grp", "fs"), ("sp", "tp"), None),
        check_vma=False,
    )
```

profile of v0, /device:TPU:33, one launch (start us, length us, event | category | flops | bytes accessed | tf_op | source)
XLA Modules:
  0.0 446.5 jit_solution(7124447785526383625)
XLA Ops:
  14.5 24.2 %all_to_all.20 = bf16[2,64,2048]{2,1,0:T(8,128)(2,1)S(1)} all-to-all(bf16[2,64,2048]{2,1,0:T(8,128)(2,1)S(1)} %broadcast_in_dim.34), channel_id=1, replica_groups=mesh['grp'=2,'sp'=16,'fs'=4,'tp'=2] {'tp'}, dimensions={0} | all-to-all | bytes 1048576 | tf_op jit(solution)/shard_map/all_to_all | solution.py:35
  39.6 3.9 all-to-all-start.2
  45.5 171.3 %all-gather.4.cloned.1.call-done = bf16[2048,4096]{1,0:T(8,128)(2,1)} async-done(((bf16[32,4096]{1,0:T(8,128)(2,1)}), bf16[2048,4096]{1,0:T(8,128)(2,1)}) %all-gather.4.cloned.1.call-update) | async-done | bytes 16777232 | tf_op jit(solution)/shard_map/all_gather | solution.py:52
  216.8 2.1 fusion.192
  219.2 2.0 fusion.191
  221.8 2.0 fusion.87
  224.9 2.0 fusion.84
  227.7 2.0 fusion.99
  229.9 2.0 fusion.93
  232.1 2.0 fusion.157
  234.1 2.0 fusion.139
  237.5 2.0 fusion.163
  239.6 2.0 fusion.151
  241.6 3.7 collective-permute-start.1
  247.1 42.4 %all-gather.8.cloned.1.call-done = bf16[2048,1024]{1,0:T(8,128)(2,1)} async-done(((bf16[128,1024]{1,0:T(8,128)(2,1)}), bf16[2048,1024]{1,0:T(8,128)(2,1)}) %all-gather.8.cloned.1.call-update) | async-done | bytes 4194320 | tf_op jit(solution)/shard_map/all_gather | solution.py:24
  289.5 3.8 fusion.188
  293.3 3.6 reshape.164
  296.9 9.1 %copy.61 = bf16[2,1024,4,2,64]{1,4,3,2,0:T(8,128)(2,1)S(1)} copy(bf16[2,1024,4,2,64]{4,3,2,1,0:T(2,128)(2,1)} %reshape.164) | data formatting | bytes 4194304
  306.0 4.0 reshape.155
  310.0 24.6 %while.31 = (s32[]{:T(128)}, f32[4,2,128]{2,1,0:T(2,128)S(1)}, f32[4,2,128]{2,1,0:T(2,128)S(1)}, f32[4,2,128,128]{3,2,1,0:T(8,128)}, s32[2]{0:T(128)S(1)}, /*ind...) while((s32[]{:T(128)}, f32[4,2,128]{2,1,0:T(2,128)S(1)}, ...), condition=%wide.region_15.16_spmd.clone, body=%wide.region_12.15_spmd.clone.sunk | while | flops 416815232 | bytes 35333296 | solution.py:130
  311.5 3.0 fusion.232
  314.5 3.3 fusion.234
  317.8 1.6 constant_dynamic-slice_fusion.5
  319.4 2.3 fusion.236
  323.2 3.0 fusion.232
  326.2 3.4 fusion.234
  329.6 1.6 constant_dynamic-slice_fusion.5
  331.3 3.3 fusion.236
  335.9 27.5 %all-gather.6.cloned.1.call-done = bf16[2048,1024]{1,0:T(8,128)(2,1)} async-done(((bf16[128,1024]{1,0:T(8,128)(2,1)}), bf16[2048,1024]{1,0:T(8,128)(2,1)}) %all-gather.6.cloned.1.call-update) | async-done | bytes 4194320 | tf_op jit(solution)/shard_map/all_gather | solution.py:24
  363.4 3.8 fusion.189
  367.2 3.6 reshape.163
  370.8 9.1 %copy.53 = bf16[2,1024,4,2,64]{1,4,3,2,0:T(8,128)(2,1)S(1)} copy(bf16[2,1024,4,2,64]{4,3,2,1,0:T(2,128)(2,1)} %reshape.163) | data formatting | bytes 4194304
  379.9 4.0 reshape.152
  383.9 22.2 %while.30 = (s32[]{:T(128)}, f32[4,2,128]{2,1,0:T(2,128)S(1)}, f32[4,2,128]{2,1,0:T(2,128)S(1)}, f32[4,2,128,128]{3,2,1,0:T(8,128)S(1)}, s32[2]{0:T(128)S(1)}, /...) while((s32[]{:T(128)}, f32[4,2,128]{2,1,0:T(2,128)S(1)}, ...), condition=%wide.region_6.7_spmd.clone, body=%wide.region_3.6_spmd.clone.sunk | while | flops 416815232 | bytes 35333296 | solution.py:130
  385.4 3.0 fusion.225
  388.3 3.3 fusion.227
  391.7 1.6 constant_dynamic-slice_fusion.4
  393.3 1.6 fusion.229
  396.4 3.0 fusion.225
  399.4 3.3 fusion.227
  402.7 1.6 constant_dynamic-slice_fusion.4
  404.3 1.6 fusion.229
  407.0 2.4 fusion.58
  409.5 4.3 fusion.40
  413.7 13.7 %all-to-all-start.1 = ((bf16[2,64,2048]{2,1,0:T(8,128)(2,1)}), bf16[2,64,2048]{2,1,0:T(8,128)(2,1)S(1)}, u32[]{:S(2)}, u32[]{:S(2)}) async-start(bf16[2,64,2048]{2,1,0:T(8,128)(2,1)} %bitcast.14), calls=%async_computation.1 | async-start | bytes 1048576 | tf_op jit(solution)/shard_map/all_to_all | solution.py:68
  427.4 2.4 fusion.56
  429.9 4.2 fusion.41
  434.1 3.5 all-to-all-start.3
  (137 shorter events, 26.9 us)
Async XLA Ops:
  6.5 38.6 %copy-start.9 = (f32[2048]{0:T(1024)S(1)}, f32[2048]{0:T(1024)}, u32[]{:S(2)}) copy-start(f32[2048]{0:T(1024)} %param.20) | copy-start | bytes 24580
  6.5 210.3 %all-gather.4.cloned.1.call-start = ((), (), s32[]{:S(2)}) async-start(), calls=%async_computation.4 | async-start | bytes 17039360 | tf_op jit(solution)/shard_map/all_gather | solution.py:52
  12.6 0.7 copy-start.6
  39.6 5.2 %all-to-all-start.2 = ((bf16[2,64,2048]{2,1,0:T(8,128)(2,1)}), bf16[2,64,2048]{2,1,0:T(8,128)(2,1)S(1)}, u32[]{:S(2)}, u32[]{:S(2)}) async-start(bf16[2,64,2048]{2,1,0:T(8,128)(2,1)} %broadcast_in_dim.35), calls=%async_computation.2 | async-start | bytes 1048576 | tf_op jit(solution)/shard_map/all_to_all | solution.py:35
  43.5 246.0 %all-gather.8.cloned.1.call-start = ((), (), s32[]{:S(2)}) async-start(), calls=%async_computation.6 | async-start | bytes 4456448 | tf_op jit(solution)/shard_map/all_gather | solution.py:24
  45.5 188.7 %copy-start.4 = (bf16[128,2048]{1,0:T(8,128)(2,1)}, bf16[128,2048]{1,0:T(8,128)(2,1)S(1)}, u32[]{:S(2)}) copy-start(bf16[128,2048]{1,0:T(8,128)(2,1)S(1)} %get-tuple-element.281) | copy-start | bytes 1572868
  45.5 194.1 %copy-start.2 = (bf16[128,2048]{1,0:T(8,128)(2,1)}, bf16[128,2048]{1,0:T(8,128)(2,1)S(1)}, u32[]{:S(2)}) copy-start(bf16[128,2048]{1,0:T(8,128)(2,1)S(1)} %get-tuple-element.280) | copy-start | bytes 1572868
  216.8 4.8 %copy-start.11 = (f32[512]{0:T(512)S(1)}, f32[512]{0:T(512)}, u32[]{:S(2)}) copy-start(f32[512]{0:T(512)} %param.25) | copy-start | bytes 6148
  221.3 3.5 copy-start.13
  221.3 3.6 copy-start.10
  224.6 138.8 %all-gather.6.cloned.1.call-start = ((), (), s32[]{:S(2)}) async-start(), calls=%async_computation.5 | async-start | bytes 4456448 | tf_op jit(solution)/shard_map/all_gather | solution.py:24
  236.2 9.4 %collective-permute-start = (bf16[2,512]{1,0:T(2,128)(2,1)S(1)}, bf16[2,512]{1,0:T(2,128)(2,1)S(1)}, u32[]{:S(2)}, u32[]{:S(2)}) collective-permute-start(bf16[2,512]{1,0:T(2,128)(2,1)S(1)} %slice.112), channel_id=1, source_target_pairs={{0,8},{8,16},{16,24},{24,32},{32,40},{40,48},{48,56},{56,64},{64,7... | collective-permute-start | bytes 6152 | tf_op jit(solution)/shard_map/ppermute | solution.py:30
  241.6 4.7 %collective-permute-start.1 = (bf16[2,512]{1,0:T(2,128)(2,1)S(1)}, bf16[2,512]{1,0:T(2,128)(2,1)S(1)}, u32[]{:S(2)}, u32[]{:S(2)}) collective-permute-start(bf16[2,512]{1,0:T(2,128)(2,1)S(1)} %slice.119), channel_id=1, source_target_pairs={{0,8},{8,16},{16,24},{24,32},{32,40},{40,48},{48,56},{56,64},{64,7... | collective-permute-start | bytes 6152 | tf_op jit(solution)/shard_map/ppermute | solution.py:30
  314.4 5.0 %copy-start = (f32[4,2,1024,128]{3,2,1,0:T(8,128)S(1)}, f32[4,2,1024,128]{3,2,1,0:T(8,128)}, u32[]{:S(2)}) copy-start(f32[4,2,1024,128]{3,2,1,0:T(8,128)} %get-tuple-element.417) | copy-start | bytes 12582916 | tf_op jit(solution)/shard_map/while
  326.2 5.0 %copy-start = (f32[4,2,1024,128]{3,2,1,0:T(8,128)S(1)}, f32[4,2,1024,128]{3,2,1,0:T(8,128)}, u32[]{:S(2)}) copy-start(f32[4,2,1024,128]{3,2,1,0:T(8,128)} %get-tuple-element.417) | copy-start | bytes 12582916 | tf_op jit(solution)/shard_map/while
  383.9 22.6 %copy-start.12 = (f32[4]{0:T(128)S(1)}, f32[4]{0:T(128)}, u32[]{:S(2)}) copy-start(f32[4]{0:T(128)} %param.26) | copy-start | bytes 52
  388.3 5.0 %copy-start.1 = (f32[4,2,1024,128]{3,2,1,0:T(8,128)S(1)}, f32[4,2,1024,128]{3,2,1,0:T(8,128)}, u32[]{:S(2)}) copy-start(f32[4,2,1024,128]{3,2,1,0:T(8,128)} %get-tuple-element.404) | copy-start | bytes 12582916 | tf_op jit(solution)/shard_map/while
  399.3 5.0 %copy-start.1 = (f32[4,2,1024,128]{3,2,1,0:T(8,128)S(1)}, f32[4,2,1024,128]{3,2,1,0:T(8,128)}, u32[]{:S(2)}) copy-start(f32[4,2,1024,128]{3,2,1,0:T(8,128)} %get-tuple-element.404) | copy-start | bytes 12582916 | tf_op jit(solution)/shard_map/while
  406.2 0.7 copy-start.14
  406.2 3.2 copy-start.8
  406.4 3.0 copy-start.5
  409.4 20.4 %copy-start.3 = (bf16[128,2048]{1,0:T(8,128)(2,1)S(1)}, bf16[128,2048]{1,0:T(8,128)(2,1)}, u32[]{:S(2)}) copy-start(bf16[128,2048]{1,0:T(8,128)(2,1)} %copy-done.2) | copy-start | bytes 1572868
  409.4 20.4 %copy-start.7 = (f32[130,512]{1,0:T(8,128)S(1)}, f32[130,512]{1,0:T(8,128)}, u32[]{:S(2)}) copy-start(f32[130,512]{1,0:T(8,128)} %maximum_convert_fusion.1) | copy-start | bytes 798724
  413.7 20.3 %all-to-all-start.1 = ((bf16[2,64,2048]{2,1,0:T(8,128)(2,1)}), bf16[2,64,2048]{2,1,0:T(8,128)(2,1)S(1)}, u32[]{:S(2)}, u32[]{:S(2)}) async-start(bf16[2,64,2048]{2,1,0:T(8,128)(2,1)} %bitcast.14), calls=%async_computation.1 | async-start | bytes 1048576 | tf_op jit(solution)/shard_map/all_to_all | solution.py:68
  434.1 4.9 %all-to-all-start.3 = ((bf16[2,64,2048]{2,1,0:T(8,128)(2,1)}), bf16[2,64,2048]{2,1,0:T(8,128)(2,1)S(1)}, u32[]{:S(2)}, u32[]{:S(2)}) async-start(bf16[2,64,2048]{2,1,0:T(8,128)(2,1)} %bitcast.25), calls=%async_computation.3 | async-start | bytes 1048576 | tf_op jit(solution)/shard_map/all_to_all | solution.py:68
Sparse Core Ops, SparseCore 0:
  13.5 203.2 all-gather.3
  224.8 64.6 all-gather.7
  291.3 72.0 all-gather.5
where the time goes:
time: 449 us; the launch traced here: 446 us
  waiting for transfers between devices  244 us (54%)
  local copies, waits for them, and re-layouts  61.3 us (14%)
  matrix products  54.4 us (12%)
  starting transfers between devices  26.2 us (6%)
  blocking collectives  24.2 us (5%)
  other arithmetic  22.5 us (5%)
  between operations  13.7 us (3%)
    all_gather x1, waiting for transfers between devices, turned_gather(): lax.all_gather(both, axis, axis=0, tiled=True)  171 us
    all_gather x2, waiting for transfers between devices, in_one_piece(): lax.all_gather(both, axis, axis=dim, tiled=True)  69.9 us
    unnamed x35, local copies, waits for them, and re-layouts  24.4 us
    all_to_all x1, blocking collectives, copy_for_each(): return lax.all_to_all(copies, axis, split_axis=0, concat_axis=0, tiled=True)  24.2 us
    all_to_all x2, starting transfers between devices, sent_and_summed(): lax.all_to_all(tiles, axis, split_axis=0, concat_axis=0, tiled=True)  17.2 us
    reduce_sum x4, other arithmetic, step(): total = total * factor + jnp.sum(weights, axis=-1)  13.4 us
    dot_general x4, matrix products, step(): jnp.einsum('qhmd,khmd->hmqk', query, key_block, preferred_element_type=jn...  11.9 us
  transfers between devices with their start and end apart: 8, of which 5 were waited for; matrix products, arithmetic and copies ran while one was open for 16% of the time, Pallas kernels for 0%

commit v1 on v0

v1 whole, which is shorter than its diff:
```python
import functools

import jax
import jax.numpy as jnp
from jax import lax
from jax.experimental import pallas as pl
from jax.experimental.pallas import tpu as pltpu
from jax.sharding import PartitionSpec as P

EPS = 1e-06
NEG = -1e30
OUT_SCALE = 0.8
HD = 128
HALF = HD // 2
PAIR = 2 * HD
TAIL = 8
F32 = jnp.float32
BF16 = jnp.bfloat16
MESH = pl.DeviceIdType.MESH


def kernel(
    n_sp,
    n_fs,
    tok_ref,
    norm_gain_ref,
    wq_ref,
    wk_ref,
    wv_ref,
    q_gain_ref,
    k_gain_ref,
    lam_ref,
    head_gain_ref,
    wb_ref,
    wc_ref,
    wi_ref,
    taps_ref,
    woa_ref,
    woc_ref,
    out_ref,
    tokens,
    stage,
    w_in,
    w_out,
    qkv,
    gate_b,
    heads,
    score,
    attn,
    attn_all,
    shaped,
    conv,
    conv_all,
    lams,
    w_send,
    w_recv,
    t_send,
    t_recv,
    ring_send,
    ring_recv,
    a_send,
    a_recv,
    kv_send,
    kv_recv,
    o_send,
    o_recv,
    c_send,
    c_recv,
    wo_send,
    wo_recv,
    one_send,
    one_recv,
):
    z, x, c = lax.axis_index("sp"), lax.axis_index("fs"), lax.axis_index("tp")
    own_seqs, rows, width = tok_ref.shape
    own_rows = own_seqs * rows
    block = 2 * rows
    keys = 2 * block
    part = wq_ref.shape[0]
    zpart = n_fs * part
    n_seq = own_seqs * n_fs
    half_ring = n_sp // 2
    xr, xl, xo = lax.rem(x + 1, n_fs), lax.rem(x + n_fs - 1, n_fs), lax.rem(x + 2, n_fs)
    zr, zl = lax.rem(z + 1, n_sp), lax.rem(z + n_sp - 1, n_sp)
    other = 1 - c
    me = n_fs * c + x

    def copy(src, dst, send, recv, **where):
        return pltpu.make_async_remote_copy(
            src_ref=src,
            dst_ref=dst,
            send_sem=send,
            recv_sem=recv,
            device_id=where,
            device_id_type=MESH,
        )

    barrier = pltpu.get_barrier_semaphore()
    near = [dict(fs=xr), dict(fs=xl), dict(fs=xo), dict(tp=other), dict(sp=zr), dict(sp=zl)]
    for where in near:
        pl.semaphore_signal(barrier, inc=1, device_id=where, device_id_type=MESH)

    sides = ((wq_ref, wk_ref), (wv_ref, wb_ref), (wc_ref, wi_ref), (woa_ref, woc_ref))
    for to in range(n_fs):
        lanes = slice(to * HD, (to + 1) * HD)
        for k, (left, right) in enumerate(sides):
            stage[to, k, :, 0:HD] = left[:, lanes]
            stage[to, k, :, HD:PAIR] = right[:, lanes]
    pl.semaphore_wait(barrier, len(near))

    here = pl.ds(pl.multiple_of(z * zpart + x * part, part), part)
    shard_copies = []
    for n, to in enumerate((xr, xl, xo)):
        shard_copies.append(
            copy(stage.at[to, 0:3], w_in.at[:, here, :], w_send.at[n, 0], w_recv.at[n, 0], fs=to)
        )
        shard_copies.append(
            copy(stage.at[to, 3], w_out.at[n_fs * c + to, here, :], w_send.at[n, 1], w_recv.at[n, 1], fs=to)
        )
    for sent in shard_copies:
        sent.start()
    w_in[:, here, :] = stage[x, 0:3]
    w_out[me, here, :] = stage[x, 3]

    step_rows = min(rows, 32)
    for s in range(own_seqs):
        for r in range(0, rows, step_rows):
            wide = tok_ref[s, r : r + step_rows, :].astype(F32)
            scale = lax.rsqrt(jnp.mean(wide * wide, axis=-1, keepdims=True) + EPS)
            at = pl.multiple_of(c * own_rows + s * rows + r, step_rows)
            tokens[x, pl.ds(at, step_rows), :] = (wide * scale * norm_gain_ref[...]).astype(BF16)

    class RowGather:
        def __init__(self, ref, size, send, recv):
            self.ref, self.size, self.send, self.recv = ref, size, send, recv

        def one(self, n, i, part_of, **where):
            first, length = ((0, self.size), (0, self.size // 2), (self.size // 2, self.size // 2))[part_of]
            ref = self.ref(i, first, length)
            return copy(ref, ref, self.send.at[n], self.recv.at[n], **where)

        def sent_as(self, n):
            i, part_of, where = (
                (x, 0, dict(fs=xr)),
                (x, 0, dict(fs=xl)),
                (xl, 1, dict(fs=xr)),
                (xr, 2, dict(fs=xl)),
                (x, 0, dict(tp=other)),
                (xl, 0, dict(tp=other)),
                (xr, 0, dict(tp=other)),
                (xo, 0, dict(tp=other)),
            )[n]
            return self.one(n, i, part_of, **where)

        def own(self):
            for n in (0, 1, 4):
                self.sent_as(n).start()

        def neighbours(self):
            self.one(0, xl, 0, fs=xr).wait_recv()
            self.sent_as(2).start()
            self.one(1, xr, 0, fs=xl).wait_recv()
            for n in (3, 5, 6):
                self.sent_as(n).start()

        def opposite(self):
            self.one(2, xo, 1, fs=xr).wait_recv()
            self.one(3, xo, 2, fs=xl).wait_recv()
            self.sent_as(7).start()

        def arrived(self, other_ref):
            mine, self.ref = self.ref, other_ref
            for n, i in ((4, x), (5, xl), (6, xr), (7, xo)):
                self.one(n, i, 0, tp=other).wait_recv()
            self.ref = mine

        def sent(self):
            for n in range(8):
                self.sent_as(n).wait_send()

    def token_ref(core):
        def ref(i, first, length):
            return tokens.at[i, pl.ds(pl.multiple_of(core * own_rows + first, length), length), :]

        return ref

    token_gather = RowGather(token_ref(c), own_rows, t_send, t_recv)
    token_gather.own()

    lane = lax.broadcasted_iota(jnp.int32, lam_ref.shape, 1)
    chosen = jnp.sum(jnp.where(lane == x, lam_ref[...], 0.0), axis=-1, keepdims=True)
    lams[c] = jnp.broadcast_to(chosen, lams.shape[1:])
    lam_copy = copy(lams.at[c], lams.at[c], one_send.at[0], one_recv.at[0], tp=other)
    lam_copy.start()

    def slice_ref(k, zb):
        at = pl.ds(pl.multiple_of(zb * zpart, zpart), zpart)
        return w_out.at[me, at, :] if k == 3 else w_in.at[k, at, :]

    def ring(way, step, k, ahead):
        if way == 0:
            zb, to = lax.rem(z - step - ahead + 2 * n_sp, n_sp), zr
        else:
            zb, to = lax.rem(z + step + ahead, n_sp), zl
        ref = slice_ref(k, zb)
        return copy(ref, ref, ring_send.at[way, step, k], ring_recv.at[way, step, k], sp=to)

    def active(way, step, k):
        return step < half_ring - 1 or (step == half_ring - 1 and (k < 2) == (way == 0))

    for n, source in enumerate((xl, xr, xo)):
        there = pl.ds(pl.multiple_of(z * zpart + source * part, part), part)
        copy(stage.at[x, 0:3], w_in.at[:, there, :], w_send.at[n, 0], w_recv.at[n, 0], fs=source).wait_recv()
        copy(stage.at[x, 3], w_out.at[me, there, :], w_send.at[n, 1], w_recv.at[n, 1], fs=source).wait_recv()
    for k in range(4):
        for way in range(2):
            ring(way, 0, k, 0).start()
    for step in range(half_ring):
        for k in range(4):
            for way in range(2):
                if active(way, step, k):
                    ring(way, step, k, 1).wait_recv()
                    if active(way, step + 1, k):
                        ring(way, step + 1, k, 0).start()
        if step == half_ring // 2 - 2:
            token_gather.neighbours()
        if step == half_ring // 2:
            token_gather.opposite()
    token_gather.arrived(token_ref(other))

    def w_out_ref(core):
        def ref(i, first, length):
            return w_out.at[n_fs * core + i, pl.ds(first, length), :]

        return ref

    w_out_gather = RowGather(w_out_ref(c), width, wo_send, wo_recv)

    lanes_x = pl.ds(pl.multiple_of(x * HD, HD), HD)
    low = lax.broadcasted_iota(jnp.int32, (2 * own_rows, HD), 1) < HALF

    def unit(raw, gain):
        wide = raw.astype(BF16).astype(F32)
        square = wide * wide
        first = jnp.sum(jnp.where(low, square, 0.0), axis=-1, keepdims=True)
        second = jnp.sum(jnp.where(low, 0.0, square), axis=-1, keepdims=True)
        scale = jnp.where(low, lax.rsqrt(first / HALF + EPS), lax.rsqrt(second / HALF + EPS))
        return wide * scale * gain

    @pl.loop(0, n_fs)
    def _(i):
        normed = tokens[i]
        both = jnp.dot(normed, w_in[0], preferred_element_type=F32)
        query = (unit(both[:, :HD], q_gain_ref[:, lanes_x]) * HALF**-0.5).astype(BF16)
        key = unit(both[:, HD:], k_gain_ref[:, lanes_x]).astype(BF16)
        both = jnp.dot(normed, w_in[1], preferred_element_type=F32).astype(BF16)
        gate_b[i] = both[:, HD:]
        for s in range(own_seqs):
            for core in range(2):
                src = slice(core * own_rows + s * rows, core * own_rows + (s + 1) * rows)
                dst = slice(core * rows, (core + 1) * rows)
                qkv[own_seqs * i + s, dst, 0:HD] = query[src]
                qkv[own_seqs * i + s, dst, HD:PAIR] = key[src]
                qkv[own_seqs * i + s, dst, PAIR:] = both[src, :HD]

    def owner(zb):
        return lax.rem(lax.rem(zb, 2) + zb // 2, 2)

    def own_block(i):
        return 2 * i + lax.rem(i + c, 2)

    def other_block(i):
        return 2 * i + lax.rem(i + other, 2)

    offsets = [n_seq // 2]
    for d in range(n_seq // 2 - 1, 0, -1):
        offsets += [d, n_seq - d]
    my_owner = owner(z)

    def qkv_copy(n, offset):
        s = lax.rem(z // 2 + offset, n_seq)
        return copy(qkv.at[s], heads.at[z], a_send.at[n], a_recv.at[z // 2], sp=2 * s + c, tp=my_owner)

    for n, offset in enumerate(offsets):
        qkv_copy(n, offset).start()
    last = len(offsets)
    home = (c == lax.rem(z, 2)) & (my_owner == c)
    away = (c != lax.rem(z, 2)) | (my_owner != c)

    @pl.when(away)
    def _():
        qkv_copy(last, 0).start()

    @pl.when(home)
    def _():
        heads[z] = qkv[z // 2]

    w_out_gather.own()

    @pl.loop(0, n_fs)
    def _(i):
        both = jnp.dot(tokens[i], w_in[2], preferred_element_type=F32).astype(BF16)
        both = both.astype(F32)
        product = (both[:, :HD] * both[:, HD:]).astype(BF16).astype(F32)
        for s in range(own_seqs):
            for core in range(2):
                src = slice(core * own_rows + s * rows, core * own_rows + (s + 1) * rows)
                shaped[own_seqs * i + s, TAIL + core * rows : TAIL + (core + 1) * rows, :] = product[src]

    tail_copy = copy(
        shaped.at[:, block : block + TAIL, :],
        shaped.at[:, 0:TAIL, :],
        one_send.at[1],
        one_recv.at[1],
        sp=zr,
    )
    tail_copy.start()
    tail_copy.wait_recv()

    @pl.when(z == 0)
    def _():
        shaped[:, 0:TAIL, :] = jnp.zeros((n_seq, TAIL, HD), F32)

    taps = [taps_ref[i : i + 1, lanes_x] for i in range(3)]

    @pl.loop(0, n_fs)
    def _(i):
        for s in range(own_seqs):
            seq = own_seqs * i + s
            total = taps[0] * shaped[seq, TAIL - 2 : TAIL - 2 + block, :]
            total = total + taps[1] * shaped[seq, TAIL - 1 : TAIL - 1 + block, :]
            total = total + taps[2] * shaped[seq, TAIL : TAIL + block, :]
            for core in range(2):
                gate = gate_b[i, core * own_rows + s * rows : core * own_rows + (s + 1) * rows, :]
                mixed = gate.astype(F32) * total[core * rows : (core + 1) * rows]
                conv[2 * i + core, s * rows : (s + 1) * rows, :] = mixed.astype(BF16)

    def conv_copy(n, to, core):
        return copy(conv.at[2 * to + core], conv_all.at[me], c_send.at[n], c_recv.at[me], fs=to, tp=core)

    conv_to = [(xo, c), (xo, other), (xr, c), (xr, other), (xl, c), (xl, other), (x, other)]
    for n, (to, core) in enumerate(conv_to):
        conv_copy(n, to, core).start()
    conv_all[me] = conv[2 * x + c]

    w_out_gather.neighbours()

    def kv_copy(i, zb):
        ref = heads.at[zb, :, HD:]
        return copy(ref, ref, kv_send.at[i], kv_recv.at[i], tp=other)

    for i in range(n_seq):
        zb = own_block(i)

        @pl.when((zb != z) | (c != lax.rem(z, 2)))
        def _():
            copy(qkv.at[0], heads.at[zb], a_send.at[0], a_recv.at[i], sp=zb, tp=c).wait_recv()

        kv_copy(i, zb).start()
    w_out_gather.opposite()
    lam_copy.wait_recv()
    for i in range(n_seq):
        kv_copy(i, other_block(i)).wait_recv()

    seq, mine = z // 2, lax.rem(z, 2)
    head = n_fs * mine + x
    seq_x, seq_row = seq // own_seqs, pl.ds(pl.multiple_of(lax.rem(seq, own_seqs) * rows, rows), rows)
    lane = lax.broadcasted_iota(jnp.int32, (block, HD), 1)
    key_at = lax.broadcasted_iota(jnp.int32, (2 * block, keys), 1)
    row_at = lax.rem(lax.broadcasted_iota(jnp.int32, (2 * block, keys), 0), block)

    def out_copy(i, zb, core):
        return copy(
            attn.at[i, core * rows : (core + 1) * rows, :],
            attn_all.at[head, seq_row, :],
            o_send.at[i, core],
            o_recv.at[head, lax.rem(seq, own_seqs)],
            fs=seq_x,
            sp=zb,
            tp=core,
        )

    def is_self(zb, core):
        return (seq_x == x) & (zb == z) & (c == core)

    def not_self(zb, core):
        return (seq_x != x) | (zb != z) | (c != core)

    def attend(i):
        zb = own_block(i)
        query = heads[zb, :, 0:HD].astype(F32)
        query = jnp.concatenate(
            [jnp.where(lane < HALF, query, 0.0), jnp.where(lane < HALF, 0.0, query)], axis=0
        ).astype(BF16)
        top = None
        for j in range(i + 1):
            key = heads[2 * j : 2 * j + 2, :, HD:PAIR].reshape(keys, HD)
            s = lax.dot_general(query, key, (((1,), (1,)), ((), ())), preferred_element_type=F32)
            if j == i:
                s = jnp.where(key_at <= row_at + block * lax.rem(i + c, 2), s, NEG)
            score[:, j * keys : (j + 1) * keys] = s
            best = functools.reduce(jnp.maximum, [s[:, n : n + HD] for n in range(0, keys, HD)] if keys >= HD else [s])
            top = best if top is None else jnp.maximum(top, best)
        top = jnp.max(top, axis=-1, keepdims=True)
        total, summed = None, None
        for j in range(i + 1):
            weight = jnp.exp(score[:, j * keys : (j + 1) * keys] - top)
            value = heads[2 * j : 2 * j + 2, :, PAIR:].reshape(keys, HD)
            add = jnp.dot(weight.astype(BF16), value, preferred_element_type=F32)
            w = sum(weight[:, n : n + HD] for n in range(0, keys, HD)) if keys >= HD else weight
            total = w if total is None else total + w
            summed = add if summed is None else summed + add
        maps = summed / jnp.sum(total, axis=-1, keepdims=True)
        differ = maps[:block] - lams[mine][0:1, :] * maps[block:]
        scale = lax.rsqrt(jnp.mean(differ * differ, axis=-1, keepdims=True) + EPS)
        attn[i] = (differ * scale * head_gain_ref[...] * OUT_SCALE).astype(BF16)
        for core in range(2):

            @pl.when(not_self(zb, core))
            def _():
                out_copy(i, zb, core).start()

            @pl.when(is_self(zb, core))
            def _():
                attn_all[head, seq_row, :] = attn[i, core * rows : (core + 1) * rows, :]

    @pl.loop(0, n_seq)
    def _(turn):
        now = lax.rem(z // 2 + turn, n_seq)
        for i in range(n_seq):

            @pl.when(now == i)
            def _():
                attend(i)

    w_out_gather.arrived(w_out_ref(other))
    for n, (to, core) in enumerate(conv_to):
        source = n_fs * core + to
        copy(conv.at[0], conv_all.at[source], c_send.at[n], c_recv.at[source], fs=to, tp=core).wait_recv()
    for h in range(2 * n_fs):
        for s in range(own_seqs):
            source_x, source_z = h % n_fs, 2 * (own_seqs * x + s) + h // n_fs

            @pl.when((source_x != x) | (source_z != z) | (my_owner != c))
            def _():
                copy(
                    attn.at[0, 0:rows, :],
                    attn_all.at[h, s * rows : (s + 1) * rows, :],
                    o_send.at[0, 0],
                    o_recv.at[h, s],
                    fs=source_x,
                    sp=source_z,
                    tp=my_owner,
                ).wait_recv()

    features = [jnp.concatenate([attn_all[h], conv_all[h]], axis=1) for h in range(2 * n_fs)]
    columns = min(width, 256)

    @pl.loop(0, width // columns)
    def _(n):
        at = pl.ds(pl.multiple_of(n * columns, columns), columns)
        total = None
        for h in range(2 * n_fs):
            add = lax.dot_general(
                features[h], w_out[h, at, :], (((1,), (1,)), ((), ())), preferred_element_type=F32
            )
            total = add if total is None else total + add
        for s in range(own_seqs):
            out_ref[s, :, at] = total[s * rows : (s + 1) * rows].astype(BF16)

    for sent in shard_copies:
        sent.wait_send()
    for step in range(half_ring):
        for k in range(4):
            for way in range(2):
                if active(way, step, k):
                    ring(way, step, k, 0).wait_send()
    token_gather.sent()
    w_out_gather.sent()
    lam_copy.wait_send()
    tail_copy.wait_send()
    for n, offset in enumerate(offsets):
        qkv_copy(n, offset).wait_send()

    @pl.when(away)
    def _():
        qkv_copy(last, 0).wait_send()

    for n, (to, core) in enumerate(conv_to):
        conv_copy(n, to, core).wait_send()
    for i in range(n_seq):
        zb = own_block(i)
        kv_copy(i, zb).wait_send()
        for core in range(2):

            @pl.when(not_self(zb, core))
            def _():
                out_copy(i, zb, core).wait_send()


def on_device(n_sp, n_fs, *args):
    tokens, norm_gain, wq, wk, wv, q_gain, k_gain, lam, head_gain, wb, wc, wi, taps, woa, woc = args
    own_seqs, rows, width = tokens.shape
    n_seq, block, n_head = own_seqs * n_fs, 2 * rows, 2 * n_fs
    assert n_sp == 2 * n_seq and n_fs == 4 and own_seqs == 2
    half_ring = n_sp // 2
    dma = pltpu.SemaphoreType.DMA
    vmem = pl.BlockSpec(memory_space=pltpu.VMEM)
    call = pl.pallas_call(
        functools.partial(kernel, n_sp, n_fs),
        out_shape=jax.ShapeDtypeStruct(tokens.shape, BF16),
        in_specs=[vmem] * 15,
        out_specs=vmem,
        scratch_shapes=[
            pltpu.VMEM((n_fs, 2 * own_seqs * rows, width), BF16),
            pltpu.VMEM((n_fs, 4, wq.shape[0], PAIR), BF16),
            pltpu.VMEM((3, width, PAIR), BF16),
            pltpu.VMEM((n_head, width, PAIR), BF16),
            pltpu.VMEM((n_seq, block, 3 * HD), BF16),
            pltpu.VMEM((n_fs, 2 * own_seqs * rows, HD), BF16),
            pltpu.VMEM((n_sp, block, 3 * HD), BF16),
            pltpu.VMEM((2 * block, n_sp * block), F32),
            pltpu.VMEM((n_seq, block, HD), BF16),
            pltpu.VMEM((n_head, own_seqs * rows, HD), BF16),
            pltpu.VMEM((n_seq, TAIL + block, HD), F32),
            pltpu.VMEM((n_head, own_seqs * rows, HD), BF16),
            pltpu.VMEM((n_head, own_seqs * rows, HD), BF16),
            pltpu.VMEM((2, 8, HD), F32),
            dma((3, 2)),
            dma((3, 2)),
            dma((8,)),
            dma((8,)),
            dma((2, half_ring, 4)),
            dma((2, half_ring, 4)),
            dma((n_seq,)),
            dma((n_seq,)),
            dma((n_seq,)),
            dma((n_seq,)),
            dma((n_seq, 2)),
            dma((n_head, own_seqs)),
            dma((n_head,)),
            dma((n_head,)),
            dma((8,)),
            dma((8,)),
            dma((2,)),
            dma((2,)),
        ],
        compiler_params=pltpu.CompilerParams(
            collective_id=0, has_side_effects=True, vmem_limit_bytes=56 * 1024 * 1024
        ),
    )
    row = lambda v: v.reshape(1, -1)
    return call(
        tokens, row(norm_gain), wq, wk, wv, row(q_gain), row(k_gain), row(lam), row(head_gain),
        wb, wc, wi, taps, woa.T, woc.T,
    )


def solution(mesh):
    placed = (
        P(("grp", "fs"), ("sp", "tp"), None),
        P(),
        P(("sp", "fs"), "tp"),
        P(("sp", "fs"), "tp"),
        P(("sp", "fs"), "tp"),
        P("tp"),
        P("tp"),
        P("tp"),
        P(),
        P(("sp", "fs"), "tp"),
        P(("sp", "fs"), "tp"),
        P(("sp", "fs"), "tp"),
        P(None, "tp"),
        P("tp", ("sp", "fs")),
        P("tp", ("sp", "fs")),
    )
    return jax.shard_map(
        functools.partial(on_device, mesh.shape["sp"], mesh.shape["fs"]),
        mesh=mesh,
        in_specs=placed,
        out_specs=P(("grp", "fs"), ("sp", "tp"), None),
        check_vma=False,
    )
```

time: 449 us -> 147 us (0.33)
  waiting for transfers between devices: 244 us -> 0 us
  Pallas kernels: 0 us -> 145 us
  local copies, waits for them, and re-layouts: 61.3 us -> 1.88 us
  matrix products: 54.4 us -> 0 us
  starting transfers between devices: 26.2 us -> 0 us
  blocking collectives: 24.2 us -> 0 us
  other arithmetic: 22.5 us -> 0 us
  between operations: 13.7 us -> 0.01 us
    all_gather x3 -> x0, waiting for transfers between devices: 241 us -> none  [the longest x1 171 us: turned_gather(): lax.all_gather(both, axis, axis=0, tiled=True)]
    pallas_call x0 -> x1, Pallas kernels: none -> 145 us  [on_device(): call(tokens, row(norm_gain), wq, wk, wv, row(q_gain), row(k_gain), row(la...]
    dot_general x22 -> x0, matrix products: 54.4 us -> none  [the longest x4 11.9 us: step(): jnp.einsum('qhmd,khmd->hmqk', query, key_block, preferred_element_type=jn...]
    all_to_all x1 -> x0, blocking collectives: 24.2 us -> none  [copy_for_each(): return lax.all_to_all(copies, axis, split_axis=0, concat_axis=0, tiled=True)]
    unnamed x35 -> x1, local copies, waits for them, and re-layouts: 24.4 us -> 1.88 us
    all_to_all x3 -> x0, starting transfers between devices: 21.1 us -> none  [the longest x2 17.2 us: sent_and_summed(): lax.all_to_all(tiles, axis, split_axis=0, concat_axis=0, tiled=True)]
    reshape x4 -> x0, local copies, waits for them, and re-layouts: 15.2 us -> none  [the longest x2 7.97 us: attend_heads(): value_blocks = value_piece.reshape(blocks, width, heads_here, DV)]
    reduce_sum x13 -> x0, other arithmetic: 14.3 us -> none  [the longest x4 13.4 us: step(): total = total * factor + jnp.sum(weights, axis=-1)]
  transfers between devices with their start and end apart: 8 -> 0, of which waited for: 5 -> 0; matrix products, arithmetic and copies ran while one was open for 16% -> 0% of each run, Pallas kernels for 0% -> 0%
where the time goes in v1:
time: 147 us
  Pallas kernels  145 us (99%)
  local copies, waits for them, and re-layouts  1.88 us (1%)
    pallas_call x1, Pallas kernels, on_device(): call(tokens, row(norm_gain), wq, wk, wv, row(q_gain), row(k_gain), row(la...  145 us

profile of v1, /device:TPU:33, one launch (start us, length us, event | category | flops | bytes accessed | tf_op | source)
XLA Modules:
  0.0 146.8 jit_solution(3351852469739453380)
XLA Ops:
  0.0 144.9 %shard_map.145 = bf16[2,64,2048]{2,1,0:T(8,128)(2,1)} custom-call(bf16[2,64,2048]{2,1,0:T(8,128)(2,1)} %tok_ref.1, f32[1,2048]{1,0:T(1,128)} %bitcast.9, bf16[32,512]{1,0:T(8,128)(2,1)} %wq_ref.1, bf16[32,512]{1,0:T(8,128)(2,1)} %wk_ref.1, bf16[32,512]{1,0:T(8,128)(2,1)} %wv_ref.1, f32[1,512]{1,0:T(1,128)} %bitcast.10, f32[1,512]{1,0:T(1,128)} %bitcast.11, ...), custom_call_target="tpu_custom_call" | custom-call | tf_op jit(solution)/shard_map/pallas_call | solution.py:553
  144.9 1.9 %copy.17 = bf16[2,64,2048]{2,1,0:T(8,128)(2,1)} copy(bf16[2,64,2048]{2,1,0:T(8,128)(2,1)} %shard_map.145) | data formatting | bytes 1048576

commit v2 on v1

--- a/solution.py
+++ b/solution.py
@@ -20,6 +20,7 @@
 
 
 def kernel(
+    n_grp,
     n_sp,
     n_fs,
     tok_ref,
@@ -40,8 +41,7 @@
     out_ref,
     tokens,
     stage,
-    w_in,
-    w_out,
+    wall,
     qkv,
     gate_b,
     heads,
@@ -58,6 +58,9 @@
     t_recv,
     ring_send,
     ring_recv,
+    pair_send,
+    pair_recv,
+    ready,
     a_send,
     a_recv,
     kv_send,
@@ -71,6 +74,7 @@
     one_send,
     one_recv,
 ):
+    g = lax.axis_index("grp")
     z, x, c = lax.axis_index("sp"), lax.axis_index("fs"), lax.axis_index("tp")
     own_seqs, rows, width = tok_ref.shape
     own_rows = own_seqs * rows
@@ -84,6 +88,9 @@
     zr, zl = lax.rem(z + 1, n_sp), lax.rem(z + n_sp - 1, n_sp)
     other = 1 - c
     me = n_fs * c + x
+    odd = lax.rem(g, 2)
+    pair = g + 1 - 2 * odd
+    out_at = 3
 
     def copy(src, dst, send, recv, **where):
         return pltpu.make_async_remote_copy(
@@ -96,7 +103,7 @@
         )
 
     barrier = pltpu.get_barrier_semaphore()
-    near = [dict(fs=xr), dict(fs=xl), dict(fs=xo), dict(tp=other), dict(sp=zr), dict(sp=zl)]
+    near = [dict(fs=xr), dict(fs=xl), dict(fs=xo), dict(tp=other), dict(sp=zl), dict(grp=pair)]
     for where in near:
         pl.semaphore_signal(barrier, inc=1, device_id=where, device_id_type=MESH)
 
@@ -108,19 +115,21 @@
             stage[to, k, :, HD:PAIR] = right[:, lanes]
     pl.semaphore_wait(barrier, len(near))
 
+    pl.semaphore_signal(ready, inc=1, device_id=dict(sp=zr), device_id_type=MESH)
+
+    def chunk_at(k, to):
+        return out_at + n_fs * c + to if k == 3 else k
+
+    def shard_copy(k, n, to, source):
+        at = pl.ds(pl.multiple_of(z * zpart + source * part, part), part)
+        return copy(stage.at[to, k], wall.at[chunk_at(k, to), at, :], w_send.at[n, k], w_recv.at[n, k], fs=to)
+
+    for k in range(4):
+        for n, to in ((2, xo), (0, xr), (1, xl)):
+            shard_copy(k, n, to, x).start()
     here = pl.ds(pl.multiple_of(z * zpart + x * part, part), part)
-    shard_copies = []
-    for n, to in enumerate((xr, xl, xo)):
-        shard_copies.append(
-            copy(stage.at[to, 0:3], w_in.at[:, here, :], w_send.at[n, 0], w_recv.at[n, 0], fs=to)
-        )
-        shard_copies.append(
-            copy(stage.at[to, 3], w_out.at[n_fs * c + to, here, :], w_send.at[n, 1], w_recv.at[n, 1], fs=to)
-        )
-    for sent in shard_copies:
-        sent.start()
-    w_in[:, here, :] = stage[x, 0:3]
-    w_out[me, here, :] = stage[x, 3]
+    wall[0:3, here, :] = stage[x, 0:3]
+    wall[out_at + me, here, :] = stage[x, 3]
 
     step_rows = min(rows, 32)
     for s in range(own_seqs):
@@ -131,13 +140,13 @@
             tokens[x, pl.ds(at, step_rows), :] = (wide * scale * norm_gain_ref[...]).astype(BF16)
 
     class RowGather:
-        def __init__(self, ref, size, send, recv):
-            self.ref, self.size, self.send, self.recv = ref, size, send, recv
+        def __init__(self, ref, size, send, recv, j):
+            self.ref, self.size, self.send, self.recv, self.j = ref, size, send, recv, j
 
         def one(self, n, i, part_of, **where):
             first, length = ((0, self.size), (0, self.size // 2), (self.size // 2, self.size // 2))[part_of]
             ref = self.ref(i, first, length)
-            return copy(ref, ref, self.send.at[n], self.recv.at[n], **where)
+            return copy(ref, ref, self.send.at[self.j, n], self.recv.at[self.j, n], **where)
 
         def sent_as(self, n):
             i, part_of, where = (
@@ -184,7 +193,7 @@
 
         return ref
 
-    token_gather = RowGather(token_ref(c), own_rows, t_send, t_recv)
+    token_gather = RowGather(token_ref(c), own_rows, t_send, t_recv, 0)
     token_gather.own()
 
     lane = lax.broadcasted_iota(jnp.int32, lam_ref.shape, 1)
@@ -193,48 +202,63 @@
     lam_copy = copy(lams.at[c], lams.at[c], one_send.at[0], one_recv.at[0], tp=other)
     lam_copy.start()
 
-    def slice_ref(k, zb):
-        at = pl.ds(pl.multiple_of(zb * zpart, zpart), zpart)
-        return w_out.at[me, at, :] if k == 3 else w_in.at[k, at, :]
+    slots = (0, 1, 2 + odd * (1 + me))
+    from_pair = 2 + (1 - odd) * (1 + me)
+
+    def slice_ref(at, zb):
+        return wall.at[at, pl.ds(pl.multiple_of(zb * zpart, zpart), zpart), :]
+
+    def ring_block(way, step):
+        return lax.rem(z - step + 2 * n_sp, n_sp) if way == 0 else lax.rem(z + step, n_sp)
 
     def ring(way, step, k, ahead):
-        if way == 0:
-            zb, to = lax.rem(z - step - ahead + 2 * n_sp, n_sp), zr
-        else:
-            zb, to = lax.rem(z + step + ahead, n_sp), zl
-        ref = slice_ref(k, zb)
+        ref = slice_ref(slots[k], ring_block(way, step + ahead))
+        to = zr if way == 0 else zl
         return copy(ref, ref, ring_send.at[way, step, k], ring_recv.at[way, step, k], sp=to)
 
+    def pair_copy(way, step, at):
+        ref = slice_ref(at, ring_block(way, step + 1))
+        return copy(ref, ref, pair_send.at[way, step], pair_recv.at[way, step], grp=pair)
+
     def active(way, step, k):
-        return step < half_ring - 1 or (step == half_ring - 1 and (k < 2) == (way == 0))
-
-    for n, source in enumerate((xl, xr, xo)):
-        there = pl.ds(pl.multiple_of(z * zpart + source * part, part), part)
-        copy(stage.at[x, 0:3], w_in.at[:, there, :], w_send.at[n, 0], w_recv.at[n, 0], fs=source).wait_recv()
-        copy(stage.at[x, 3], w_out.at[me, there, :], w_send.at[n, 1], w_recv.at[n, 1], fs=source).wait_recv()
+        return step < half_ring - 1 or (step == half_ring - 1 and (k == 0) == (way == 0))
+
+    hops = [(way, step) for step in range(half_ring) for way in range(2) if active(way, step, 2)]
+
     for k in range(4):
-        for way in range(2):
-            ring(way, 0, k, 0).start()
+        for n, source in ((2, xo), (0, xl), (1, xr)):
+            shard_copy(k, n, x, source).wait_recv()
+        for slot, its in enumerate(((0,), (1,), (2, 3))):
+            if k == its[-1]:
+                ring(0, 0, slot, 0).start()
+    pl.semaphore_wait(ready, 1)
+    for k in range(3):
+        ring(1, 0, k, 0).start()
     for step in range(half_ring):
-        for k in range(4):
+        for k in range(3):
             for way in range(2):
                 if active(way, step, k):
                     ring(way, step, k, 1).wait_recv()
                     if active(way, step + 1, k):
                         ring(way, step + 1, k, 0).start()
-        if step == half_ring // 2 - 2:
+                    if k == 2:
+                        pair_copy(way, step, slots[2]).start()
+        if step == 2:
             token_gather.neighbours()
-        if step == half_ring // 2:
+        if step == 4:
             token_gather.opposite()
     token_gather.arrived(token_ref(other))
 
-    def w_out_ref(core):
+    pieces = wo_send.shape[0]
+    piece = width // pieces
+
+    def w_out_ref(core, j):
         def ref(i, first, length):
-            return w_out.at[n_fs * core + i, pl.ds(first, length), :]
+            return wall.at[out_at + n_fs * core + i, pl.ds(j * piece + first, length), :]
 
         return ref
 
-    w_out_gather = RowGather(w_out_ref(c), width, wo_send, wo_recv)
+    w_out_gathers = [RowGather(w_out_ref(c, j), piece, wo_send, wo_recv, j) for j in range(pieces)]
 
     lanes_x = pl.ds(pl.multiple_of(x * HD, HD), HD)
     low = lax.broadcasted_iota(jnp.int32, (2 * own_rows, HD), 1) < HALF
@@ -250,10 +274,10 @@
     @pl.loop(0, n_fs)
     def _(i):
         normed = tokens[i]
-        both = jnp.dot(normed, w_in[0], preferred_element_type=F32)
+        both = jnp.dot(normed, wall[0], preferred_element_type=F32)
         query = (unit(both[:, :HD], q_gain_ref[:, lanes_x]) * HALF**-0.5).astype(BF16)
         key = unit(both[:, HD:], k_gain_ref[:, lanes_x]).astype(BF16)
-        both = jnp.dot(normed, w_in[1], preferred_element_type=F32).astype(BF16)
+        both = jnp.dot(normed, wall[1], preferred_element_type=F32).astype(BF16)
         gate_b[i] = both[:, HD:]
         for s in range(own_seqs):
             for core in range(2):
@@ -295,11 +319,14 @@
     def _():
         heads[z] = qkv[z // 2]
 
-    w_out_gather.own()
+    for way, step in hops:
+        pair_copy(way, step, from_pair).wait_recv()
+    for gather in w_out_gathers:
+        gather.own()
 
     @pl.loop(0, n_fs)
     def _(i):
-        both = jnp.dot(tokens[i], w_in[2], preferred_element_type=F32).astype(BF16)
+        both = jnp.dot(tokens[i], wall[2], preferred_element_type=F32).astype(BF16)
         both = both.astype(F32)
         product = (both[:, :HD] * both[:, HD:]).astype(BF16).astype(F32)
         for s in range(own_seqs):
@@ -315,35 +342,8 @@
         sp=zr,
     )
     tail_copy.start()
-    tail_copy.wait_recv()
-
-    @pl.when(z == 0)
-    def _():
-        shaped[:, 0:TAIL, :] = jnp.zeros((n_seq, TAIL, HD), F32)
-
-    taps = [taps_ref[i : i + 1, lanes_x] for i in range(3)]
-
-    @pl.loop(0, n_fs)
-    def _(i):
-        for s in range(own_seqs):
-            seq = own_seqs * i + s
-            total = taps[0] * shaped[seq, TAIL - 2 : TAIL - 2 + block, :]
-            total = total + taps[1] * shaped[seq, TAIL - 1 : TAIL - 1 + block, :]
-            total = total + taps[2] * shaped[seq, TAIL : TAIL + block, :]
-            for core in range(2):
-                gate = gate_b[i, core * own_rows + s * rows : core * own_rows + (s + 1) * rows, :]
-                mixed = gate.astype(F32) * total[core * rows : (core + 1) * rows]
-                conv[2 * i + core, s * rows : (s + 1) * rows, :] = mixed.astype(BF16)
-
-    def conv_copy(n, to, core):
-        return copy(conv.at[2 * to + core], conv_all.at[me], c_send.at[n], c_recv.at[me], fs=to, tp=core)
-
-    conv_to = [(xo, c), (xo, other), (xr, c), (xr, other), (xl, c), (xl, other), (x, other)]
-    for n, (to, core) in enumerate(conv_to):
-        conv_copy(n, to, core).start()
-    conv_all[me] = conv[2 * x + c]
-
-    w_out_gather.neighbours()
+    for gather in w_out_gathers:
+        gather.neighbours()
 
     def kv_copy(i, zb):
         ref = heads.at[zb, :, HD:]
@@ -357,7 +357,6 @@
             copy(qkv.at[0], heads.at[zb], a_send.at[0], a_recv.at[i], sp=zb, tp=c).wait_recv()
 
         kv_copy(i, zb).start()
-    w_out_gather.opposite()
     lam_copy.wait_recv()
     for i in range(n_seq):
         kv_copy(i, other_block(i)).wait_recv()
@@ -433,7 +432,39 @@
             def _():
                 attend(i)
 
-    w_out_gather.arrived(w_out_ref(other))
+    for gather in w_out_gathers:
+        gather.opposite()
+    tail_copy.wait_recv()
+
+    @pl.when(z == 0)
+    def _():
+        shaped[:, 0:TAIL, :] = jnp.zeros((n_seq, TAIL, HD), F32)
+
+    taps = [taps_ref[i : i + 1, lanes_x] for i in range(3)]
+
+    @pl.loop(0, n_fs)
+    def _(i):
+        for s in range(own_seqs):
+            seq = own_seqs * i + s
+            total = taps[0] * shaped[seq, TAIL - 2 : TAIL - 2 + block, :]
+            total = total + taps[1] * shaped[seq, TAIL - 1 : TAIL - 1 + block, :]
+            total = total + taps[2] * shaped[seq, TAIL : TAIL + block, :]
+            for core in range(2):
+                gate = gate_b[i, core * own_rows + s * rows : core * own_rows + (s + 1) * rows, :]
+                mixed = gate.astype(F32) * total[core * rows : (core + 1) * rows]
+                conv[2 * i + core, s * rows : (s + 1) * rows, :] = mixed.astype(BF16)
+
+    def conv_copy(n, to, core):
+        return copy(conv.at[2 * to + core], conv_all.at[me], c_send.at[n], c_recv.at[me], fs=to, tp=core)
+
+    conv_to = [(xo, c), (xo, other), (xr, c), (xr, other), (xl, c), (xl, other), (x, other)]
+    for n, (to, core) in enumerate(conv_to):
+        conv_copy(n, to, core).start()
+    conv_all[me] = conv[2 * x + c]
+
+
+    for j, gather in enumerate(w_out_gathers):
+        gather.arrived(w_out_ref(other, j))
     for n, (to, core) in enumerate(conv_to):
         source = n_fs * core + to
         copy(conv.at[0], conv_all.at[source], c_send.at[n], c_recv.at[source], fs=to, tp=core).wait_recv()
@@ -462,21 +493,25 @@
         total = None
         for h in range(2 * n_fs):
             add = lax.dot_general(
-                features[h], w_out[h, at, :], (((1,), (1,)), ((), ())), preferred_element_type=F32
+                features[h], wall[out_at + h, at, :], (((1,), (1,)), ((), ())), preferred_element_type=F32
             )
             total = add if total is None else total + add
         for s in range(own_seqs):
             out_ref[s, :, at] = total[s * rows : (s + 1) * rows].astype(BF16)
 
-    for sent in shard_copies:
-        sent.wait_send()
+    for k in range(4):
+        for n, to in enumerate((xr, xl, xo)):
+            shard_copy(k, n, to, x).wait_send()
+    for way, step in hops:
+        pair_copy(way, step, slots[2]).wait_send()
     for step in range(half_ring):
-        for k in range(4):
+        for k in range(3):
             for way in range(2):
                 if active(way, step, k):
                     ring(way, step, k, 0).wait_send()
     token_gather.sent()
-    w_out_gather.sent()
+    for gather in w_out_gathers:
+        gather.sent()
     lam_copy.wait_send()
     tail_copy.wait_send()
     for n, offset in enumerate(offsets):
@@ -498,24 +533,23 @@
                 out_copy(i, zb, core).wait_send()
 
 
-def on_device(n_sp, n_fs, *args):
+def on_device(n_grp, n_sp, n_fs, *args):
     tokens, norm_gain, wq, wk, wv, q_gain, k_gain, lam, head_gain, wb, wc, wi, taps, woa, woc = args
     own_seqs, rows, width = tokens.shape
     n_seq, block, n_head = own_seqs * n_fs, 2 * rows, 2 * n_fs
-    assert n_sp == 2 * n_seq and n_fs == 4 and own_seqs == 2
+    assert n_grp % 2 == 0 and n_sp == 2 * n_seq and n_fs == 4 and own_seqs == 2
     half_ring = n_sp // 2
     dma = pltpu.SemaphoreType.DMA
     vmem = pl.BlockSpec(memory_space=pltpu.VMEM)
     call = pl.pallas_call(
-        functools.partial(kernel, n_sp, n_fs),
+        functools.partial(kernel, n_grp, n_sp, n_fs),
         out_shape=jax.ShapeDtypeStruct(tokens.shape, BF16),
         in_specs=[vmem] * 15,
         out_specs=vmem,
         scratch_shapes=[
             pltpu.VMEM((n_fs, 2 * own_seqs * rows, width), BF16),
             pltpu.VMEM((n_fs, 4, wq.shape[0], PAIR), BF16),
-            pltpu.VMEM((3, width, PAIR), BF16),
-            pltpu.VMEM((n_head, width, PAIR), BF16),
+            pltpu.VMEM((3 + n_head, width, PAIR), BF16),
             pltpu.VMEM((n_seq, block, 3 * HD), BF16),
             pltpu.VMEM((n_fs, 2 * own_seqs * rows, HD), BF16),
             pltpu.VMEM((n_sp, block, 3 * HD), BF16),
@@ -526,12 +560,15 @@
             pltpu.VMEM((n_head, own_seqs * rows, HD), BF16),
             pltpu.VMEM((n_head, own_seqs * rows, HD), BF16),
             pltpu.VMEM((2, 8, HD), F32),
-            dma((3, 2)),
-            dma((3, 2)),
-            dma((8,)),
-            dma((8,)),
-            dma((2, half_ring, 4)),
-            dma((2, half_ring, 4)),
+            dma((3, 4)),
+            dma((3, 4)),
+            dma((1, 8)),
+            dma((1, 8)),
+            dma((2, half_ring, 3)),
+            dma((2, half_ring, 3)),
+            dma((2, half_ring)),
+            dma((2, half_ring)),
+            pltpu.SemaphoreType.REGULAR,
             dma((n_seq,)),
             dma((n_seq,)),
             dma((n_seq,)),
@@ -540,8 +577,8 @@
             dma((n_head, own_seqs)),
             dma((n_head,)),
             dma((n_head,)),
-            dma((8,)),
-            dma((8,)),
+            dma((4, 8)),
+            dma((4, 8)),
             dma((2,)),
             dma((2,)),
         ],
@@ -575,7 +612,7 @@
         P("tp", ("sp", "fs")),
     )
     return jax.shard_map(
-        functools.partial(on_device, mesh.shape["sp"], mesh.shape["fs"]),
+        functools.partial(on_device, mesh.shape["grp"], mesh.shape["sp"], mesh.shape["fs"]),
         mesh=mesh,
         in_specs=placed,
         out_specs=P(("grp", "fs"), ("sp", "tp"), None),

time: 147 us -> 130 us (0.88)
  Pallas kernels: 145 us -> 128 us
    pallas_call x1, Pallas kernels: 145 us -> 128 us  [on_device(): call(tokens, row(norm_gain), wq, wk, wv, row(q_gain), row(k_gain), row(la...]
where the time goes in v2:
time: 130 us
  Pallas kernels  128 us (98%)
  local copies, waits for them, and re-layouts  1.88 us (1%)
    pallas_call x1, Pallas kernels, on_device(): call(tokens, row(norm_gain), wq, wk, wv, row(q_gain), row(k_gain), row(la...  128 us

profile of v2, /device:TPU:33, one launch (start us, length us, event | category | flops | bytes accessed | tf_op | source)
XLA Modules:
  0.0 129.8 jit_solution(8809917539228773133)
XLA Ops:
  0.0 127.9 %shard_map.145 = bf16[2,64,2048]{2,1,0:T(8,128)(2,1)} custom-call(bf16[2,64,2048]{2,1,0:T(8,128)(2,1)} %tok_ref.1, f32[1,2048]{1,0:T(1,128)} %bitcast.9, bf16[32,512]{1,0:T(8,128)(2,1)} %wq_ref.1, bf16[32,512]{1,0:T(8,128)(2,1)} %wk_ref.1, bf16[32,512]{1,0:T(8,128)(2,1)} %wv_ref.1, f32[1,512]{1,0:T(1,128)} %bitcast.10, f32[1,512]{1,0:T(1,128)} %bitcast.11, ...), custom_call_target="tpu_custom_call" | custom-call | tf_op jit(solution)/shard_map/pallas_call | solution.py:590
  127.9 1.9 %copy.17 = bf16[2,64,2048]{2,1,0:T(8,128)(2,1)} copy(bf16[2,64,2048]{2,1,0:T(8,128)(2,1)} %shard_map.145) | data formatting | bytes 1048576

commit v3 on v2

--- a/solution.py
+++ b/solution.py
@@ -23,25 +23,15 @@
     n_grp,
     n_sp,
     n_fs,
-    tok_ref,
-    norm_gain_ref,
-    wq_ref,
-    wk_ref,
-    wv_ref,
-    q_gain_ref,
-    k_gain_ref,
-    lam_ref,
-    head_gain_ref,
-    wb_ref,
-    wc_ref,
-    wi_ref,
-    taps_ref,
-    woa_ref,
-    woc_ref,
+    *refs,
+):
+    (tok_ref, norm_gain_ref, wq_ref, wk_ref, wv_ref, q_gain_ref, k_gain_ref, lam_ref, head_gain_ref, wb_ref, wc_ref, wi_ref, taps_ref, woa_ref, woc_ref) = refs[16:31]
+    (
     out_ref,
     tokens,
     stage,
     wall,
+    partial,
     qkv,
     gate_b,
     heads,
@@ -52,6 +42,7 @@
     conv,
     conv_all,
     lams,
+    mixed,
     w_send,
     w_recv,
     t_send,
@@ -73,7 +64,11 @@
     wo_recv,
     one_send,
     one_recv,
-):
+    load_sem,
+    ) = (refs[15], *refs[31:])
+    loads = [pltpu.make_async_copy(refs[n], refs[16 + n], load_sem.at[n]) for n in range(15)]
+    for n in (2, 3, 4, 9, 10, 11, 13, 14, 0, 1, 5, 6, 7, 8, 12):
+        loads[n].start()
     g = lax.axis_index("grp")
     z, x, c = lax.axis_index("sp"), lax.axis_index("fs"), lax.axis_index("tp")
     own_seqs, rows, width = tok_ref.shape
@@ -107,6 +102,9 @@
     for where in near:
         pl.semaphore_signal(barrier, inc=1, device_id=where, device_id_type=MESH)
 
+    for n in range(15):
+        loads[n].wait()
+
     sides = ((wq_ref, wk_ref), (wv_ref, wb_ref), (wc_ref, wi_ref), (woa_ref, woc_ref))
     for to in range(n_fs):
         lanes = slice(to * HD, (to + 1) * HD)
@@ -202,52 +200,89 @@
     lam_copy = copy(lams.at[c], lams.at[c], one_send.at[0], one_recv.at[0], tp=other)
     lam_copy.start()
 
-    slots = (0, 1, 2 + odd * (1 + me))
-    from_pair = 2 + (1 - odd) * (1 + me)
-
-    def slice_ref(at, zb):
-        return wall.at[at, pl.ds(pl.multiple_of(zb * zpart, zpart), zpart), :]
+    def slice_ref(k, zb, side):
+        first = zb * zpart
+        if k == 3:
+            first, length = first + side * (zpart // 2), zpart // 2
+        else:
+            length = zpart
+        at = pl.ds(pl.multiple_of(first, length), length)
+        if k == 2:
+            return wall.at[2 + side * (1 + me), at, :]
+        return wall.at[(0, 1, 2, 1)[k], at, (slice(0, PAIR), slice(0, HD), None, slice(HD, PAIR))[k]]
 
     def ring_block(way, step):
         return lax.rem(z - step + 2 * n_sp, n_sp) if way == 0 else lax.rem(z + step, n_sp)
 
     def ring(way, step, k, ahead):
-        ref = slice_ref(slots[k], ring_block(way, step + ahead))
+        ref = slice_ref(k, ring_block(way, step + ahead), odd)
         to = zr if way == 0 else zl
         return copy(ref, ref, ring_send.at[way, step, k], ring_recv.at[way, step, k], sp=to)
 
-    def pair_copy(way, step, at):
-        ref = slice_ref(at, ring_block(way, step + 1))
-        return copy(ref, ref, pair_send.at[way, step], pair_recv.at[way, step], grp=pair)
+    def pair_copy(way, step, k, side):
+        ref = slice_ref(k, ring_block(way, step + 1), side)
+        return copy(ref, ref, pair_send.at[k - 2, way, step], pair_recv.at[k - 2, way, step], grp=pair)
 
     def active(way, step, k):
-        return step < half_ring - 1 or (step == half_ring - 1 and (k == 0) == (way == 0))
-
-    hops = [(way, step) for step in range(half_ring) for way in range(2) if active(way, step, 2)]
+        return step < half_ring - 1 or (step == half_ring - 1 and (k in (0, 3)) == (way == 0))
+
+    hops = [(way, step, k) for step in range(half_ring) for k in (2, 3) for way in range(2) if active(way, step, k)]
+
+    @pl.when(z != 0)
+    def _():
+        pl.semaphore_wait(ready, 1)
 
     for k in range(4):
         for n, source in ((2, xo), (0, xl), (1, xr)):
             shard_copy(k, n, x, source).wait_recv()
-        for slot, its in enumerate(((0,), (1,), (2, 3))):
-            if k == its[-1]:
+        for slot, its in enumerate((0, 1, 3, 1)):
+            if k == its:
                 ring(0, 0, slot, 0).start()
-    pl.semaphore_wait(ready, 1)
-    for k in range(3):
-        ring(1, 0, k, 0).start()
+
+                @pl.when(z != 0)
+                def _():
+                    ring(1, 0, slot, 0).start()
+
+    @pl.when(z == 0)
+    def _():
+        pl.semaphore_wait(ready, 1)
+        for k in range(4):
+            ring(1, 0, k, 0).start()
+
+    def project(i, blocks, first=False):
+        for k in range(2):
+            lanes = slice(0, PAIR if k == 0 else HD)
+            total = None if first else partial[k, i, :, lanes]
+            for zb in blocks:
+                at = pl.ds(pl.multiple_of(zb * zpart, zpart), zpart)
+                add = jnp.dot(tokens[i, :, at], wall[k, at, lanes], preferred_element_type=F32)
+                total = add if total is None else total + add
+            partial[k, i, :, lanes] = total
+
+    def blocks_of(steps):
+        return [ring_block(way, step + 1) for step in steps for way in range(2)]
+
+    late = half_ring - 3
     for step in range(half_ring):
-        for k in range(3):
+        for k in range(4):
             for way in range(2):
                 if active(way, step, k):
                     ring(way, step, k, 1).wait_recv()
                     if active(way, step + 1, k):
                         ring(way, step + 1, k, 0).start()
-                    if k == 2:
-                        pair_copy(way, step, slots[2]).start()
+                    if k >= 2:
+                        pair_copy(way, step, k, odd).start()
+            if step == late:
+                project(k, [z] + blocks_of(range(late)), first=True)
+            elif step > late:
+                project(k, blocks_of((step - 1,)))
         if step == 2:
             token_gather.neighbours()
         if step == 4:
             token_gather.opposite()
-    token_gather.arrived(token_ref(other))
+        if step == late - 1:
+            token_gather.arrived(token_ref(other))
+    last_block = [ring_block(0, half_ring)]
 
     pieces = wo_send.shape[0]
     piece = width // pieces
@@ -271,21 +306,19 @@
         scale = jnp.where(low, lax.rsqrt(first / HALF + EPS), lax.rsqrt(second / HALF + EPS))
         return wide * scale * gain
 
-    @pl.loop(0, n_fs)
-    def _(i):
-        normed = tokens[i]
-        both = jnp.dot(normed, wall[0], preferred_element_type=F32)
+    for i in range(n_fs):
+        project(i, last_block)
+        both = partial[0, i]
         query = (unit(both[:, :HD], q_gain_ref[:, lanes_x]) * HALF**-0.5).astype(BF16)
         key = unit(both[:, HD:], k_gain_ref[:, lanes_x]).astype(BF16)
-        both = jnp.dot(normed, wall[1], preferred_element_type=F32).astype(BF16)
-        gate_b[i] = both[:, HD:]
+        value = partial[1, i, :, 0:HD].astype(BF16)
         for s in range(own_seqs):
             for core in range(2):
                 src = slice(core * own_rows + s * rows, core * own_rows + (s + 1) * rows)
                 dst = slice(core * rows, (core + 1) * rows)
                 qkv[own_seqs * i + s, dst, 0:HD] = query[src]
                 qkv[own_seqs * i + s, dst, HD:PAIR] = key[src]
-                qkv[own_seqs * i + s, dst, PAIR:] = both[src, :HD]
+                qkv[own_seqs * i + s, dst, PAIR:] = value[src]
 
     def owner(zb):
         return lax.rem(lax.rem(zb, 2) + zb // 2, 2)
@@ -319,8 +352,8 @@
     def _():
         heads[z] = qkv[z // 2]
 
-    for way, step in hops:
-        pair_copy(way, step, from_pair).wait_recv()
+    for way, step, k in hops:
+        pair_copy(way, step, k, 1 - odd).wait_recv()
     for gather in w_out_gathers:
         gather.own()
 
@@ -328,6 +361,7 @@
     def _(i):
         both = jnp.dot(tokens[i], wall[2], preferred_element_type=F32).astype(BF16)
         both = both.astype(F32)
+        gate_b[i] = jnp.dot(tokens[i], wall[1, :, HD:PAIR], preferred_element_type=F32).astype(BF16)
         product = (both[:, :HD] * both[:, HD:]).astype(BF16).astype(F32)
         for s in range(own_seqs):
             for core in range(2):
@@ -345,6 +379,35 @@
     for gather in w_out_gathers:
         gather.neighbours()
 
+    tail_copy.wait_recv()
+
+    @pl.when(z == 0)
+    def _():
+        shaped[:, 0:TAIL, :] = jnp.zeros((n_seq, TAIL, HD), F32)
+
+    taps = [taps_ref[i : i + 1, lanes_x] for i in range(3)]
+
+    @pl.loop(0, n_fs)
+    def _(i):
+        for s in range(own_seqs):
+            seq = own_seqs * i + s
+            total = taps[0] * shaped[seq, TAIL - 2 : TAIL - 2 + block, :]
+            total = total + taps[1] * shaped[seq, TAIL - 1 : TAIL - 1 + block, :]
+            total = total + taps[2] * shaped[seq, TAIL : TAIL + block, :]
+            for core in range(2):
+                gate = gate_b[i, core * own_rows + s * rows : core * own_rows + (s + 1) * rows, :]
+                gated = gate.astype(F32) * total[core * rows : (core + 1) * rows]
+                conv[2 * i + core, s * rows : (s + 1) * rows, :] = gated.astype(BF16)
+
+    def conv_copy(n, to, core):
+        return copy(conv.at[2 * to + core], conv_all.at[me], c_send.at[n], c_recv.at[me], fs=to, tp=core)
+
+    conv_to = [(xo, c), (xo, other), (xr, c), (xr, other), (xl, c), (xl, other), (x, other)]
+    for n, (to, core) in enumerate(conv_to):
+        conv_copy(n, to, core).start()
+    conv_all[me] = conv[2 * x + c]
+
+
     def kv_copy(i, zb):
         ref = heads.at[zb, :, HD:]
         return copy(ref, ref, kv_send.at[i], kv_recv.at[i], tp=other)
@@ -357,6 +420,8 @@
             copy(qkv.at[0], heads.at[zb], a_send.at[0], a_recv.at[i], sp=zb, tp=c).wait_recv()
 
         kv_copy(i, zb).start()
+    for gather in w_out_gathers[:-1]:
+        gather.opposite()
     lam_copy.wait_recv()
     for i in range(n_seq):
         kv_copy(i, other_block(i)).wait_recv()
@@ -432,42 +497,32 @@
             def _():
                 attend(i)
 
-    for gather in w_out_gathers:
-        gather.opposite()
-    tail_copy.wait_recv()
-
-    @pl.when(z == 0)
-    def _():
-        shaped[:, 0:TAIL, :] = jnp.zeros((n_seq, TAIL, HD), F32)
-
-    taps = [taps_ref[i : i + 1, lanes_x] for i in range(3)]
-
-    @pl.loop(0, n_fs)
-    def _(i):
-        for s in range(own_seqs):
-            seq = own_seqs * i + s
-            total = taps[0] * shaped[seq, TAIL - 2 : TAIL - 2 + block, :]
-            total = total + taps[1] * shaped[seq, TAIL - 1 : TAIL - 1 + block, :]
-            total = total + taps[2] * shaped[seq, TAIL : TAIL + block, :]
-            for core in range(2):
-                gate = gate_b[i, core * own_rows + s * rows : core * own_rows + (s + 1) * rows, :]
-                mixed = gate.astype(F32) * total[core * rows : (core + 1) * rows]
-                conv[2 * i + core, s * rows : (s + 1) * rows, :] = mixed.astype(BF16)
-
-    def conv_copy(n, to, core):
-        return copy(conv.at[2 * to + core], conv_all.at[me], c_send.at[n], c_recv.at[me], fs=to, tp=core)
-
-    conv_to = [(xo, c), (xo, other), (xr, c), (xr, other), (xl, c), (xl, other), (x, other)]
-    for n, (to, core) in enumerate(conv_to):
-        conv_copy(n, to, core).start()
-    conv_all[me] = conv[2 * x + c]
-
-
+    w_out_gathers[-1].opposite()
     for j, gather in enumerate(w_out_gathers):
         gather.arrived(w_out_ref(other, j))
     for n, (to, core) in enumerate(conv_to):
         source = n_fs * core + to
         copy(conv.at[0], conv_all.at[source], c_send.at[n], c_recv.at[source], fs=to, tp=core).wait_recv()
+    columns = min(width, 256)
+
+    def projected(features, lanes, at):
+        total = None
+        for h in range(0, 2 * n_fs, 2):
+            weight = jnp.concatenate([wall[out_at + h, at, lanes], wall[out_at + h + 1, at, lanes]], axis=1)
+            add = lax.dot_general(
+                jnp.concatenate([features[h], features[h + 1]], axis=1),
+                weight,
+                (((1,), (1,)), ((), ())),
+                preferred_element_type=F32,
+            )
+            total = add if total is None else total + add
+        return total
+
+    @pl.loop(0, width // columns)
+    def _(n):
+        at = pl.ds(pl.multiple_of(n * columns, columns), columns)
+        mixed[:, at] = projected(conv_all, slice(HD, PAIR), at)
+
     for h in range(2 * n_fs):
         for s in range(own_seqs):
             source_x, source_z = h % n_fs, 2 * (own_seqs * x + s) + h // n_fs
@@ -484,28 +539,20 @@
                     tp=my_owner,
                 ).wait_recv()
 
-    features = [jnp.concatenate([attn_all[h], conv_all[h]], axis=1) for h in range(2 * n_fs)]
-    columns = min(width, 256)
-
     @pl.loop(0, width // columns)
     def _(n):
         at = pl.ds(pl.multiple_of(n * columns, columns), columns)
-        total = None
-        for h in range(2 * n_fs):
-            add = lax.dot_general(
-                features[h], wall[out_at + h, at, :], (((1,), (1,)), ((), ())), preferred_element_type=F32
-            )
-            total = add if total is None else total + add
+        total = mixed[:, at] + projected(attn_all, slice(0, HD), at)
         for s in range(own_seqs):
             out_ref[s, :, at] = total[s * rows : (s + 1) * rows].astype(BF16)
 
     for k in range(4):
         for n, to in enumerate((xr, xl, xo)):
             shard_copy(k, n, to, x).wait_send()
-    for way, step in hops:
-        pair_copy(way, step, slots[2]).wait_send()
+    for way, step, k in hops:
+        pair_copy(way, step, k, odd).wait_send()
     for step in range(half_ring):
-        for k in range(3):
+        for k in range(4):
             for way in range(2):
                 if active(way, step, k):
                     ring(way, step, k, 0).wait_send()
@@ -539,17 +586,24 @@
     n_seq, block, n_head = own_seqs * n_fs, 2 * rows, 2 * n_fs
     assert n_grp % 2 == 0 and n_sp == 2 * n_seq and n_fs == 4 and own_seqs == 2
     half_ring = n_sp // 2
+    row = lambda v: v.reshape(1, -1)
+    ins = (
+        tokens, row(norm_gain), wq, wk, wv, row(q_gain), row(k_gain), row(lam), row(head_gain),
+        wb, wc, wi, taps, woa.T, woc.T,
+    )
     dma = pltpu.SemaphoreType.DMA
     vmem = pl.BlockSpec(memory_space=pltpu.VMEM)
     call = pl.pallas_call(
         functools.partial(kernel, n_grp, n_sp, n_fs),
         out_shape=jax.ShapeDtypeStruct(tokens.shape, BF16),
-        in_specs=[vmem] * 15,
+        in_specs=[pl.BlockSpec(memory_space=pltpu.HBM)] * 15,
         out_specs=vmem,
-        scratch_shapes=[
+        scratch_shapes=[pltpu.VMEM(a.shape, a.dtype) for a in ins]
+        + [
             pltpu.VMEM((n_fs, 2 * own_seqs * rows, width), BF16),
             pltpu.VMEM((n_fs, 4, wq.shape[0], PAIR), BF16),
             pltpu.VMEM((3 + n_head, width, PAIR), BF16),
+            pltpu.VMEM((2, n_fs, 2 * own_seqs * rows, PAIR), F32),
             pltpu.VMEM((n_seq, block, 3 * HD), BF16),
             pltpu.VMEM((n_fs, 2 * own_seqs * rows, HD), BF16),
             pltpu.VMEM((n_sp, block, 3 * HD), BF16),
@@ -560,14 +614,15 @@
             pltpu.VMEM((n_head, own_seqs * rows, HD), BF16),
             pltpu.VMEM((n_head, own_seqs * rows, HD), BF16),
             pltpu.VMEM((2, 8, HD), F32),
+            pltpu.VMEM((own_seqs * rows, width), F32),
             dma((3, 4)),
             dma((3, 4)),
             dma((1, 8)),
             dma((1, 8)),
-            dma((2, half_ring, 3)),
-            dma((2, half_ring, 3)),
-            dma((2, half_ring)),
-            dma((2, half_ring)),
+            dma((2, half_ring, 4)),
+            dma((2, half_ring, 4)),
+            dma((2, 2, half_ring)),
+            dma((2, 2, half_ring)),
             pltpu.SemaphoreType.REGULAR,
             dma((n_seq,)),
             dma((n_seq,)),
@@ -581,16 +636,13 @@
             dma((4, 8)),
             dma((2,)),
             dma((2,)),
+            dma((15,)),
         ],
         compiler_params=pltpu.CompilerParams(
-            collective_id=0, has_side_effects=True, vmem_limit_bytes=56 * 1024 * 1024
+            collective_id=0, has_side_effects=True, vmem_limit_bytes=32 * 1024 * 1024
         ),
     )
-    row = lambda v: v.reshape(1, -1)
-    return call(
-        tokens, row(norm_gain), wq, wk, wv, row(q_gain), row(k_gain), row(lam), row(head_gain),
-        wb, wc, wi, taps, woa.T, woc.T,
-    )
+    return call(*[pltpu.with_memory_space_constraint(a, pltpu.HBM) for a in ins])
 
 
 def solution(mesh):

time: 130 us -> 128 us (0.985)
  no operation moved by 1% of the time
where the time goes in v3:
time: 128 us
  Pallas kernels  127 us (99%)
    pallas_call x1, Pallas kernels, on_device(): call(*[pltpu.with_memory_space_constraint(a, pltpu.HBM) for a in ins])  127 us

profile of v3, /device:TPU:33, one launch (start us, length us, event | category | flops | bytes accessed | tf_op | source)
XLA Modules:
  0.0 127.5 jit_solution(2756885301065863362)
XLA Ops:
  0.0 126.7 %shard_map.145 = bf16[2,64,2048]{2,1,0:T(8,128)(2,1)S(1)} custom-call(bf16[2,64,2048]{2,1,0:T(8,128)(2,1)} %refs_0_.1, f32[1,2048]{1,0:T(1,128)} %bitcast.9, bf16[32,512]{1,0:T(8,128)(2,1)} %refs_2_.1, bf16[32,512]{1,0:T(8,128)(2,1)} %refs_3_.1, bf16[32,512]{1,0:T(8,128)(2,1)} %refs_4_.1, f32[1,512]{1,0:T(1,128)} %bitcast.10, f32[1,512]{1,0:T(1,128)} %bitcast.11, ...), custom_call_target="tpu_custom_call" | custom-call | tf_op jit(solution)/shard_map/pallas_call | solution.py:645
  126.7 0.8 copy.17

commit v4 on v3

--- a/solution.py
+++ b/solution.py
@@ -43,31 +43,25 @@
     conv_all,
     lams,
     mixed,
-    w_send,
+    send,
     w_recv,
-    t_send,
     t_recv,
-    ring_send,
     ring_recv,
-    pair_send,
     pair_recv,
     ready,
-    a_send,
     a_recv,
-    kv_send,
     kv_recv,
-    o_send,
     o_recv,
-    c_send,
     c_recv,
-    wo_send,
     wo_recv,
     one_send,
     one_recv,
     load_sem,
     ) = (refs[15], *refs[31:])
-    loads = [pltpu.make_async_copy(refs[n], refs[16 + n], load_sem.at[n]) for n in range(15)]
-    for n in (2, 3, 4, 9, 10, 11, 13, 14, 0, 1, 5, 6, 7, 8, 12):
+    weights, others = (2, 3, 4, 9, 10, 11, 13, 14), (0, 1, 5, 6, 7, 8, 12)
+    load_at = {n: 0 for n in weights} | {n: 1 + i for i, n in enumerate(others)}
+    loads = [pltpu.make_async_copy(refs[n], refs[16 + n], load_sem.at[load_at[n]]) for n in range(15)]
+    for n in weights + others:
         loads[n].start()
     g = lax.axis_index("grp")
     z, x, c = lax.axis_index("sp"), lax.axis_index("fs"), lax.axis_index("tp")
@@ -97,12 +91,25 @@
             device_id_type=MESH,
         )
 
+    def together(sem, size):
+        lines = size // (2 * PAIR)
+        for most in range(1, wall.shape[0] + 1):
+            if lines % most == 0 and lines // most <= width and lines // most % 16 == 0:
+                ref = wall.at[0:most, 0 : lines // most, :]
+                return copy(ref, ref, sem, sem, tp=other)
+        raise ValueError(size)
+
+    shard_size, slice_size = part * 2 * PAIR, zpart * 2 * PAIR
+    token_size, conv_size = own_rows * width * 2, own_rows * HD * 2
+    out_size, kv_size = rows * HD * 2, block * 2 * PAIR
+
     barrier = pltpu.get_barrier_semaphore()
     near = [dict(fs=xr), dict(fs=xl), dict(fs=xo), dict(tp=other), dict(sp=zl), dict(grp=pair)]
     for where in near:
         pl.semaphore_signal(barrier, inc=1, device_id=where, device_id_type=MESH)
 
-    for n in range(15):
+    pltpu.make_async_copy(stage, stage, load_sem.at[0]).wait()
+    for n in others:
         loads[n].wait()
 
     sides = ((wq_ref, wk_ref), (wv_ref, wb_ref), (wc_ref, wi_ref), (woa_ref, woc_ref))
@@ -120,7 +127,7 @@
 
     def shard_copy(k, n, to, source):
         at = pl.ds(pl.multiple_of(z * zpart + source * part, part), part)
-        return copy(stage.at[to, k], wall.at[chunk_at(k, to), at, :], w_send.at[n, k], w_recv.at[n, k], fs=to)
+        return copy(stage.at[to, k], wall.at[chunk_at(k, to), at, :], send.at[0], w_recv.at[k], fs=to)
 
     for k in range(4):
         for n, to in ((2, xo), (0, xr), (1, xl)):
@@ -144,7 +151,7 @@
         def one(self, n, i, part_of, **where):
             first, length = ((0, self.size), (0, self.size // 2), (self.size // 2, self.size // 2))[part_of]
             ref = self.ref(i, first, length)
-            return copy(ref, ref, self.send.at[self.j, n], self.recv.at[self.j, n], **where)
+            return copy(ref, ref, self.send, self.recv.at[self.j if n < 4 else 0, min(n, 4)], **where)
 
         def sent_as(self, n):
             i, part_of, where = (
@@ -175,24 +182,13 @@
             self.one(3, xo, 2, fs=xl).wait_recv()
             self.sent_as(7).start()
 
-        def arrived(self, other_ref):
-            mine, self.ref = self.ref, other_ref
-            for n, i in ((4, x), (5, xl), (6, xr), (7, xo)):
-                self.one(n, i, 0, tp=other).wait_recv()
-            self.ref = mine
-
-        def sent(self):
-            for n in range(8):
-                self.sent_as(n).wait_send()
-
     def token_ref(core):
         def ref(i, first, length):
             return tokens.at[i, pl.ds(pl.multiple_of(core * own_rows + first, length), length), :]
 
         return ref
 
-    token_gather = RowGather(token_ref(c), own_rows, t_send, t_recv, 0)
-    token_gather.own()
+    token_gather = RowGather(token_ref(c), own_rows, send.at[1], t_recv, 0)
 
     lane = lax.broadcasted_iota(jnp.int32, lam_ref.shape, 1)
     chosen = jnp.sum(jnp.where(lane == x, lam_ref[...], 0.0), axis=-1, keepdims=True)
@@ -200,16 +196,16 @@
     lam_copy = copy(lams.at[c], lams.at[c], one_send.at[0], one_recv.at[0], tp=other)
     lam_copy.start()
 
+    pieces_of = ((0, 0, 2), (0, 1, 2), (1, 0, 1), (2, 0, 2), (2, 1, 2), (3, 0, 2))
+
     def slice_ref(k, zb, side):
-        first = zb * zpart
-        if k == 3:
-            first, length = first + side * (zpart // 2), zpart // 2
-        else:
-            length = zpart
+        kind, nth, count = pieces_of[k]
+        length = zpart // count
+        first = zb * zpart + (side if kind == 3 else nth) * length
         at = pl.ds(pl.multiple_of(first, length), length)
-        if k == 2:
+        if kind == 2:
             return wall.at[2 + side * (1 + me), at, :]
-        return wall.at[(0, 1, 2, 1)[k], at, (slice(0, PAIR), slice(0, HD), None, slice(HD, PAIR))[k]]
+        return wall.at[(0, 1, 2, 1)[kind], at, (slice(0, PAIR), slice(0, HD), None, slice(HD, PAIR))[kind]]
 
     def ring_block(way, step):
         return lax.rem(z - step + 2 * n_sp, n_sp) if way == 0 else lax.rem(z + step, n_sp)
@@ -217,25 +213,22 @@
     def ring(way, step, k, ahead):
         ref = slice_ref(k, ring_block(way, step + ahead), odd)
         to = zr if way == 0 else zl
-        return copy(ref, ref, ring_send.at[way, step, k], ring_recv.at[way, step, k], sp=to)
+        return copy(ref, ref, send.at[2], ring_recv.at[way, step, k], sp=to)
 
     def pair_copy(way, step, k, side):
         ref = slice_ref(k, ring_block(way, step + 1), side)
-        return copy(ref, ref, pair_send.at[k - 2, way, step], pair_recv.at[k - 2, way, step], grp=pair)
+        return copy(ref, ref, send.at[3], pair_recv.at[k // 5], grp=pair)
 
     def active(way, step, k):
-        return step < half_ring - 1 or (step == half_ring - 1 and (k in (0, 3)) == (way == 0))
-
-    hops = [(way, step, k) for step in range(half_ring) for k in (2, 3) for way in range(2) if active(way, step, k)]
+        return step < half_ring - 1 or (step == half_ring - 1 and (k in (0, 1, 5)) == (way == 0))
 
     @pl.when(z != 0)
     def _():
         pl.semaphore_wait(ready, 1)
 
     for k in range(4):
-        for n, source in ((2, xo), (0, xl), (1, xr)):
-            shard_copy(k, n, x, source).wait_recv()
-        for slot, its in enumerate((0, 1, 3, 1)):
+        together(w_recv.at[k], 3 * shard_size).wait_recv()
+        for slot, its in enumerate((0, 0, 1, 3, 3, 1)):
             if k == its:
                 ring(0, 0, slot, 0).start()
 
@@ -243,10 +236,11 @@
                 def _():
                     ring(1, 0, slot, 0).start()
 
+    token_gather.own()
     @pl.when(z == 0)
     def _():
         pl.semaphore_wait(ready, 1)
-        for k in range(4):
+        for k in range(6):
             ring(1, 0, k, 0).start()
 
     def project(i, blocks, first=False):
@@ -264,27 +258,29 @@
 
     late = half_ring - 3
     for step in range(half_ring):
-        for k in range(4):
+        for k in range(6):
             for way in range(2):
                 if active(way, step, k):
                     ring(way, step, k, 1).wait_recv()
                     if active(way, step + 1, k):
                         ring(way, step + 1, k, 0).start()
-                    if k >= 2:
+                    if k >= 3:
                         pair_copy(way, step, k, odd).start()
+            if k >= n_fs:
+                continue
             if step == late:
                 project(k, [z] + blocks_of(range(late)), first=True)
             elif step > late:
                 project(k, blocks_of((step - 1,)))
-        if step == 2:
+        if step == 3:
             token_gather.neighbours()
         if step == 4:
             token_gather.opposite()
         if step == late - 1:
-            token_gather.arrived(token_ref(other))
+            together(t_recv.at[0, 4], n_fs * token_size).wait_recv()
     last_block = [ring_block(0, half_ring)]
 
-    pieces = wo_send.shape[0]
+    pieces = wo_recv.shape[0]
     piece = width // pieces
 
     def w_out_ref(core, j):
@@ -293,7 +289,7 @@
 
         return ref
 
-    w_out_gathers = [RowGather(w_out_ref(c, j), piece, wo_send, wo_recv, j) for j in range(pieces)]
+    w_out_gathers = [RowGather(w_out_ref(c, j), piece, send.at[5], wo_recv, j) for j in range(pieces)]
 
     lanes_x = pl.ds(pl.multiple_of(x * HD, HD), HD)
     low = lax.broadcasted_iota(jnp.int32, (2 * own_rows, HD), 1) < HALF
@@ -334,13 +330,14 @@
         offsets += [d, n_seq - d]
     my_owner = owner(z)
 
+    last = len(offsets)
+
     def qkv_copy(n, offset):
         s = lax.rem(z // 2 + offset, n_seq)
-        return copy(qkv.at[s], heads.at[z], a_send.at[n], a_recv.at[z // 2], sp=2 * s + c, tp=my_owner)
+        return copy(qkv.at[s], heads.at[z], send.at[4 if n < last else 9], a_recv.at[z // 2], sp=2 * s + c, tp=my_owner)
 
     for n, offset in enumerate(offsets):
         qkv_copy(n, offset).start()
-    last = len(offsets)
     home = (c == lax.rem(z, 2)) & (my_owner == c)
     away = (c != lax.rem(z, 2)) | (my_owner != c)
 
@@ -352,8 +349,8 @@
     def _():
         heads[z] = qkv[z // 2]
 
-    for way, step, k in hops:
-        pair_copy(way, step, k, 1 - odd).wait_recv()
+    together(pair_recv.at[0], (n_sp - 1) * slice_size).wait_recv()
+    together(pair_recv.at[1], (n_sp - 1) * slice_size // 4).wait_recv()
     for gather in w_out_gathers:
         gather.own()
 
@@ -379,6 +376,18 @@
     for gather in w_out_gathers:
         gather.neighbours()
 
+    def kv_copy(i, zb):
+        ref = heads.at[zb, :, HD:]
+        return copy(ref, ref, send.at[7], kv_recv.at[0], tp=other)
+
+    for i in range(n_seq):
+        zb = own_block(i)
+
+        @pl.when((zb != z) | (c != lax.rem(z, 2)))
+        def _():
+            copy(qkv.at[0], heads.at[zb], send.at[4], a_recv.at[i], sp=zb, tp=c).wait_recv()
+
+        kv_copy(i, zb).start()
     tail_copy.wait_recv()
 
     @pl.when(z == 0)
@@ -400,7 +409,7 @@
                 conv[2 * i + core, s * rows : (s + 1) * rows, :] = gated.astype(BF16)
 
     def conv_copy(n, to, core):
-        return copy(conv.at[2 * to + core], conv_all.at[me], c_send.at[n], c_recv.at[me], fs=to, tp=core)
+        return copy(conv.at[2 * to + core], conv_all.at[me], send.at[6], c_recv.at[0], fs=to, tp=core)
 
     conv_to = [(xo, c), (xo, other), (xr, c), (xr, other), (xl, c), (xl, other), (x, other)]
     for n, (to, core) in enumerate(conv_to):
@@ -408,23 +417,10 @@
     conv_all[me] = conv[2 * x + c]
 
 
-    def kv_copy(i, zb):
-        ref = heads.at[zb, :, HD:]
-        return copy(ref, ref, kv_send.at[i], kv_recv.at[i], tp=other)
-
-    for i in range(n_seq):
-        zb = own_block(i)
-
-        @pl.when((zb != z) | (c != lax.rem(z, 2)))
-        def _():
-            copy(qkv.at[0], heads.at[zb], a_send.at[0], a_recv.at[i], sp=zb, tp=c).wait_recv()
-
-        kv_copy(i, zb).start()
     for gather in w_out_gathers[:-1]:
         gather.opposite()
     lam_copy.wait_recv()
-    for i in range(n_seq):
-        kv_copy(i, other_block(i)).wait_recv()
+    together(kv_recv.at[0], n_seq * kv_size).wait_recv()
 
     seq, mine = z // 2, lax.rem(z, 2)
     head = n_fs * mine + x
@@ -437,8 +433,8 @@
         return copy(
             attn.at[i, core * rows : (core + 1) * rows, :],
             attn_all.at[head, seq_row, :],
-            o_send.at[i, core],
-            o_recv.at[head, lax.rem(seq, own_seqs)],
+            send.at[8],
+            o_recv.at[head // 2],
             fs=seq_x,
             sp=zb,
             tp=core,
@@ -450,7 +446,7 @@
     def not_self(zb, core):
         return (seq_x != x) | (zb != z) | (c != core)
 
-    def attend(i):
+    def scored(i, first):
         zb = own_block(i)
         query = heads[zb, :, 0:HD].astype(F32)
         query = jnp.concatenate(
@@ -462,22 +458,34 @@
             s = lax.dot_general(query, key, (((1,), (1,)), ((), ())), preferred_element_type=F32)
             if j == i:
                 s = jnp.where(key_at <= row_at + block * lax.rem(i + c, 2), s, NEG)
-            score[:, j * keys : (j + 1) * keys] = s
-            best = functools.reduce(jnp.maximum, [s[:, n : n + HD] for n in range(0, keys, HD)] if keys >= HD else [s])
-            top = best if top is None else jnp.maximum(top, best)
-        top = jnp.max(top, axis=-1, keepdims=True)
+            score[:, first + j * keys : first + (j + 1) * keys] = s
+            top = folded(jnp.maximum, s, top)
+        return jnp.max(top, axis=-1, keepdims=True)
+
+    def folded(op, s, start):
+        for n in range(0, keys, min(HD, keys)):
+            piece = s[:, n : n + min(HD, keys)]
+            start = piece if start is None else op(start, piece)
+        return start
+
+    def weighted(i, first, top):
         total, summed = None, None
         for j in range(i + 1):
-            weight = jnp.exp(score[:, j * keys : (j + 1) * keys] - top)
+            weight = jnp.exp(score[:, first + j * keys : first + (j + 1) * keys] - top)
             value = heads[2 * j : 2 * j + 2, :, PAIR:].reshape(keys, HD)
             add = jnp.dot(weight.astype(BF16), value, preferred_element_type=F32)
-            w = sum(weight[:, n : n + HD] for n in range(0, keys, HD)) if keys >= HD else weight
-            total = w if total is None else total + w
+            total = folded(jnp.add, weight, total)
             summed = add if summed is None else summed + add
-        maps = summed / jnp.sum(total, axis=-1, keepdims=True)
+        return summed, jnp.sum(total, axis=-1, keepdims=True)
+
+    def finished(i, summed, total):
+        maps = summed / total
         differ = maps[:block] - lams[mine][0:1, :] * maps[block:]
         scale = lax.rsqrt(jnp.mean(differ * differ, axis=-1, keepdims=True) + EPS)
         attn[i] = (differ * scale * head_gain_ref[...] * OUT_SCALE).astype(BF16)
+
+    def deliver(i):
+        zb = own_block(i)
         for core in range(2):
 
             @pl.when(not_self(zb, core))
@@ -488,96 +496,89 @@
             def _():
                 attn_all[head, seq_row, :] = attn[i, core * rows : (core + 1) * rows, :]
 
-    @pl.loop(0, n_seq)
+    @pl.loop(0, n_seq // 2)
     def _(turn):
-        now = lax.rem(z // 2 + turn, n_seq)
-        for i in range(n_seq):
-
-            @pl.when(now == i)
+        now = lax.rem(z // 2 + turn, n_seq // 2)
+        for p in range(n_seq // 2):
+
+            @pl.when(now == p)
             def _():
-                attend(i)
+                both = ((n_seq - 1 - p, 0), (p, n_sp * block))
+                tops = [scored(i, first) for i, first in both]
+                sums = [weighted(i, first, top) for (i, first), top in zip(both, tops)]
+                for (i, _), (summed, total) in zip(both, sums):
+                    finished(i, summed, total)
+                for i, _ in both:
+                    deliver(i)
 
     w_out_gathers[-1].opposite()
-    for j, gather in enumerate(w_out_gathers):
-        gather.arrived(w_out_ref(other, j))
-    for n, (to, core) in enumerate(conv_to):
-        source = n_fs * core + to
-        copy(conv.at[0], conv_all.at[source], c_send.at[n], c_recv.at[source], fs=to, tp=core).wait_recv()
+    together(wo_recv.at[0, 4], n_fs * width * 2 * PAIR).wait_recv()
+    together(c_recv.at[0], len(conv_to) * conv_size).wait_recv()
     columns = min(width, 256)
 
-    def projected(features, lanes, at):
-        total = None
-        for h in range(0, 2 * n_fs, 2):
-            weight = jnp.concatenate([wall[out_at + h, at, lanes], wall[out_at + h + 1, at, lanes]], axis=1)
-            add = lax.dot_general(
-                jnp.concatenate([features[h], features[h + 1]], axis=1),
-                weight,
-                (((1,), (1,)), ((), ())),
-                preferred_element_type=F32,
-            )
-            total = add if total is None else total + add
-        return total
+    def projected(features, lanes, at, h):
+        weight = jnp.concatenate([wall[out_at + h, at, lanes], wall[out_at + h + 1, at, lanes]], axis=1)
+        pair_of = jnp.concatenate([features[h], features[h + 1]], axis=1)
+        return lax.dot_general(pair_of, weight, (((1,), (1,)), ((), ())), preferred_element_type=F32)
+
+    def column(n):
+        return pl.ds(pl.multiple_of(n * columns, columns), columns)
 
     @pl.loop(0, width // columns)
     def _(n):
-        at = pl.ds(pl.multiple_of(n * columns, columns), columns)
-        mixed[:, at] = projected(conv_all, slice(HD, PAIR), at)
-
-    for h in range(2 * n_fs):
-        for s in range(own_seqs):
-            source_x, source_z = h % n_fs, 2 * (own_seqs * x + s) + h // n_fs
-
-            @pl.when((source_x != x) | (source_z != z) | (my_owner != c))
-            def _():
-                copy(
-                    attn.at[0, 0:rows, :],
-                    attn_all.at[h, s * rows : (s + 1) * rows, :],
-                    o_send.at[0, 0],
-                    o_recv.at[h, s],
-                    fs=source_x,
-                    sp=source_z,
-                    tp=my_owner,
-                ).wait_recv()
+        at = column(n)
+        mixed[:, at] = sum(projected(conv_all, slice(HD, PAIR), at, h) for h in range(0, 2 * n_fs, 2))
+
+    kept = (seq_x == x) & (my_owner == c)
+    sent_all = (seq_x != x) | (my_owner != c)
+    for h in range(0, 2 * n_fs, 2):
+        here_too = kept & (head // 2 == h // 2)
+        not_here = sent_all | (head // 2 != h // 2)
+
+        @pl.when(here_too)
+        def _():
+            together(o_recv.at[h // 2], (2 * own_seqs - 1) * out_size).wait_recv()
+
+        @pl.when(not_here)
+        def _():
+            together(o_recv.at[h // 2], 2 * own_seqs * out_size).wait_recv()
+
+        if h < 2 * n_fs - 2:
+
+            @pl.loop(0, width // columns)
+            def _(n):
+                at = column(n)
+                mixed[:, at] += projected(attn_all, slice(0, HD), at, h)
 
     @pl.loop(0, width // columns)
     def _(n):
-        at = pl.ds(pl.multiple_of(n * columns, columns), columns)
-        total = mixed[:, at] + projected(attn_all, slice(0, HD), at)
+        at = column(n)
+        total = mixed[:, at] + projected(attn_all, slice(0, HD), at, 2 * n_fs - 2)
         for s in range(own_seqs):
             out_ref[s, :, at] = total[s * rows : (s + 1) * rows].astype(BF16)
 
-    for k in range(4):
-        for n, to in enumerate((xr, xl, xo)):
-            shard_copy(k, n, to, x).wait_send()
-    for way, step, k in hops:
-        pair_copy(way, step, k, odd).wait_send()
-    for step in range(half_ring):
-        for k in range(4):
-            for way in range(2):
-                if active(way, step, k):
-                    ring(way, step, k, 0).wait_send()
-    token_gather.sent()
-    for gather in w_out_gathers:
-        gather.sent()
+    together(send.at[0], 12 * shard_size).wait_send()
+    together(send.at[1], 7 * token_size).wait_send()
+    together(send.at[2], (n_sp - 1) * slice_size * 11 // 4).wait_send()
+    together(send.at[3], (n_sp - 1) * slice_size * 5 // 4).wait_send()
+    together(send.at[4], last * block * 6 * HD).wait_send()
+    together(send.at[5], 7 * width * 2 * PAIR).wait_send()
+    together(send.at[6], len(conv_to) * conv_size).wait_send()
+    together(send.at[7], n_seq * kv_size).wait_send()
     lam_copy.wait_send()
     tail_copy.wait_send()
-    for n, offset in enumerate(offsets):
-        qkv_copy(n, offset).wait_send()
 
     @pl.when(away)
     def _():
         qkv_copy(last, 0).wait_send()
 
-    for n, (to, core) in enumerate(conv_to):
-        conv_copy(n, to, core).wait_send()
-    for i in range(n_seq):
-        zb = own_block(i)
-        kv_copy(i, zb).wait_send()
-        for core in range(2):
-
-            @pl.when(not_self(zb, core))
-            def _():
-                out_copy(i, zb, core).wait_send()
+    @pl.when(kept)
+    def _():
+        together(send.at[8], (2 * n_seq - 1) * out_size).wait_send()
+
+    @pl.when(sent_all)
+    def _():
+        together(send.at[8], 2 * n_seq * out_size).wait_send()
 
 
 def on_device(n_grp, n_sp, n_fs, *args):
@@ -607,7 +608,7 @@
             pltpu.VMEM((n_seq, block, 3 * HD), BF16),
             pltpu.VMEM((n_fs, 2 * own_seqs * rows, HD), BF16),
             pltpu.VMEM((n_sp, block, 3 * HD), BF16),
-            pltpu.VMEM((2 * block, n_sp * block), F32),
+            pltpu.VMEM((2 * block, n_sp * block * 3 // 2), F32),
             pltpu.VMEM((n_seq, block, HD), BF16),
             pltpu.VMEM((n_head, own_seqs * rows, HD), BF16),
             pltpu.VMEM((n_seq, TAIL + block, HD), F32),
@@ -615,28 +616,20 @@
             pltpu.VMEM((n_head, own_seqs * rows, HD), BF16),
             pltpu.VMEM((2, 8, HD), F32),
             pltpu.VMEM((own_seqs * rows, width), F32),
-            dma((3, 4)),
-            dma((3, 4)),
-            dma((1, 8)),
-            dma((1, 8)),
-            dma((2, half_ring, 4)),
-            dma((2, half_ring, 4)),
-            dma((2, 2, half_ring)),
-            dma((2, 2, half_ring)),
+            dma((10,)),
+            dma((4,)),
+            dma((1, 5)),
+            dma((2, half_ring, 6)),
+            dma((2,)),
             pltpu.SemaphoreType.REGULAR,
             dma((n_seq,)),
-            dma((n_seq,)),
-            dma((n_seq,)),
-            dma((n_seq,)),
-            dma((n_seq, 2)),
-            dma((n_head, own_seqs)),
-            dma((n_head,)),
-            dma((n_head,)),
-            dma((4, 8)),
-            dma((4, 8)),
+            dma((1,)),
+            dma((n_fs,)),
+            dma((1,)),
+            dma((4, 5)),
             dma((2,)),
             dma((2,)),
-            dma((15,)),
+            dma((8,)),
         ],
         compiler_params=pltpu.CompilerParams(
             collective_id=0, has_side_effects=True, vmem_limit_bytes=32 * 1024 * 1024

time: 128 us -> 126 us (0.984)
  Pallas kernels: 127 us -> 125 us
    pallas_call x1, Pallas kernels: 127 us -> 125 us  [on_device(): call(*[pltpu.with_memory_space_constraint(a, pltpu.HBM) for a in ins])]
where the time goes in v4:
time: 126 us
  Pallas kernels  125 us (99%)
    pallas_call x1, Pallas kernels, on_device(): call(*[pltpu.with_memory_space_constraint(a, pltpu.HBM) for a in ins])  125 us

profile of v4, /device:TPU:33, one launch (start us, length us, event | category | flops | bytes accessed | tf_op | source)
XLA Modules:
  0.0 126.1 jit_solution(2533582184063786023)
XLA Ops:
  0.0 125.3 %shard_map.145 = bf16[2,64,2048]{2,1,0:T(8,128)(2,1)S(1)} custom-call(bf16[2,64,2048]{2,1,0:T(8,128)(2,1)} %refs_0_.1, f32[1,2048]{1,0:T(1,128)} %bitcast.9, bf16[32,512]{1,0:T(8,128)(2,1)} %refs_2_.1, bf16[32,512]{1,0:T(8,128)(2,1)} %refs_3_.1, bf16[32,512]{1,0:T(8,128)(2,1)} %refs_4_.1, f32[1,512]{1,0:T(1,128)} %bitcast.10, f32[1,512]{1,0:T(1,128)} %bitcast.11, ...), custom_call_target="tpu_custom_call" | custom-call | tf_op jit(solution)/shard_map/pallas_call | solution.py:638
  125.3 0.8 copy.17

commit v5 on v4

--- a/solution.py
+++ b/solution.py
@@ -13,6 +13,7 @@
 HD = 128
 HALF = HD // 2
 PAIR = 2 * HD
+LATE = 2
 TAIL = 8
 F32 = jnp.float32
 BF16 = jnp.bfloat16
@@ -256,7 +257,7 @@
     def blocks_of(steps):
         return [ring_block(way, step + 1) for step in steps for way in range(2)]
 
-    late = half_ring - 3
+    late = half_ring - LATE
     for step in range(half_ring):
         for k in range(6):
             for way in range(2):
@@ -268,16 +269,16 @@
                         pair_copy(way, step, k, odd).start()
             if k >= n_fs:
                 continue
-            if step == late:
-                project(k, [z] + blocks_of(range(late)), first=True)
-            elif step > late:
+            if step > late:
                 project(k, blocks_of((step - 1,)))
-        if step == 3:
+        if step == late - 2:
             token_gather.neighbours()
-        if step == 4:
+        if step == late - 1:
             token_gather.opposite()
-        if step == late - 1:
+        if step == late:
             together(t_recv.at[0, 4], n_fs * token_size).wait_recv()
+            for i in range(n_fs):
+                project(i, [z] + blocks_of(range(late)), first=True)
     last_block = [ring_block(0, half_ring)]
 
     pieces = wo_recv.shape[0]
@@ -496,9 +497,16 @@
             def _():
                 attn_all[head, seq_row, :] = attn[i, core * rows : (core + 1) * rows, :]
 
+    side = jnp.minimum(seq, n_seq - 1 - seq)
+
     @pl.loop(0, n_seq // 2)
     def _(turn):
-        now = lax.rem(z // 2 + turn, n_seq // 2)
+        late_turn = turn // 2
+        inner = side // 2
+        first = n_seq // 2 - 1 - side
+        now = (1 - late_turn) * (first + lax.rem(turn, 2) * (1 - 2 * lax.rem(first, 2))) + late_turn * (
+            inner * turn + (1 - inner) * (n_seq // 2 - 1 - turn)
+        )
         for p in range(n_seq // 2):
 
             @pl.when(now == p)

time: 126 us -> 124 us (0.984)
  Pallas kernels: 125 us -> 123 us
    pallas_call x1, Pallas kernels: 125 us -> 123 us  [on_device(): call(*[pltpu.with_memory_space_constraint(a, pltpu.HBM) for a in ins])]
where the time goes in v5:
time: 124 us
  Pallas kernels  123 us (99%)
    pallas_call x1, Pallas kernels, on_device(): call(*[pltpu.with_memory_space_constraint(a, pltpu.HBM) for a in ins])  123 us

profile of v5, /device:TPU:33, one launch (start us, length us, event | category | flops | bytes accessed | tf_op | source)
XLA Modules:
  0.0 124.1 jit_solution(8378896469208564612)
XLA Ops:
  0.0 123.3 %shard_map.145 = bf16[2,64,2048]{2,1,0:T(8,128)(2,1)S(1)} custom-call(bf16[2,64,2048]{2,1,0:T(8,128)(2,1)} %refs_0_.1, f32[1,2048]{1,0:T(1,128)} %bitcast.9, bf16[32,512]{1,0:T(8,128)(2,1)} %refs_2_.1, bf16[32,512]{1,0:T(8,128)(2,1)} %refs_3_.1, bf16[32,512]{1,0:T(8,128)(2,1)} %refs_4_.1, f32[1,512]{1,0:T(1,128)} %bitcast.10, f32[1,512]{1,0:T(1,128)} %bitcast.11, ...), custom_call_target="tpu_custom_call" | custom-call | tf_op jit(solution)/shard_map/pallas_call | solution.py:646
  123.3 0.8 copy.17

commit v6 on v5

--- a/solution.py
+++ b/solution.py
@@ -13,7 +13,6 @@
 HD = 128
 HALF = HD // 2
 PAIR = 2 * HD
-LATE = 2
 TAIL = 8
 F32 = jnp.float32
 BF16 = jnp.bfloat16
@@ -197,13 +196,12 @@
     lam_copy = copy(lams.at[c], lams.at[c], one_send.at[0], one_recv.at[0], tp=other)
     lam_copy.start()
 
-    pieces_of = ((0, 0, 2), (0, 1, 2), (1, 0, 1), (2, 0, 2), (2, 1, 2), (3, 0, 2))
+    pieces_of = ((0, 0), (1, 0), (2, 0), (2, 1), (3, 0))
 
     def slice_ref(k, zb, side):
-        kind, nth, count = pieces_of[k]
-        length = zpart // count
-        first = zb * zpart + (side if kind == 3 else nth) * length
-        at = pl.ds(pl.multiple_of(first, length), length)
+        kind, nth = pieces_of[k]
+        length = zpart // 2
+        at = pl.ds(pl.multiple_of(zb * zpart + (nth if kind == 2 else side) * length, length), length)
         if kind == 2:
             return wall.at[2 + side * (1 + me), at, :]
         return wall.at[(0, 1, 2, 1)[kind], at, (slice(0, PAIR), slice(0, HD), None, slice(HD, PAIR))[kind]]
@@ -216,12 +214,22 @@
         to = zr if way == 0 else zl
         return copy(ref, ref, send.at[2], ring_recv.at[way, step, k], sp=to)
 
+    soon = half_ring - 3
+
     def pair_copy(way, step, k, side):
         ref = slice_ref(k, ring_block(way, step + 1), side)
-        return copy(ref, ref, send.at[3], pair_recv.at[k // 5], grp=pair)
+        recv = pair_recv.at[6 if k == 4 else 0 if step < soon else 1]
+        return copy(ref, ref, send.at[3], recv, grp=pair)
+
+    pieces = wo_recv.shape[0]
+    piece = width // pieces
+
+    def pair_piece(j, side):
+        ref = wall.at[2 + side * (1 + me), pl.ds(j * piece, piece), :]
+        return copy(ref, ref, send.at[3], pair_recv.at[2 + j], grp=pair)
 
     def active(way, step, k):
-        return step < half_ring - 1 or (step == half_ring - 1 and (k in (0, 1, 5)) == (way == 0))
+        return step < half_ring - 1 or (step == half_ring - 1 and (k in (0, 2)) == (way == 0))
 
     @pl.when(z != 0)
     def _():
@@ -229,7 +237,7 @@
 
     for k in range(4):
         together(w_recv.at[k], 3 * shard_size).wait_recv()
-        for slot, its in enumerate((0, 0, 1, 3, 3, 1)):
+        for slot, its in enumerate((0, 1, 3, 3, 1)):
             if k == its:
                 ring(0, 0, slot, 0).start()
 
@@ -241,7 +249,7 @@
     @pl.when(z == 0)
     def _():
         pl.semaphore_wait(ready, 1)
-        for k in range(6):
+        for k in range(5):
             ring(1, 0, k, 0).start()
 
     def project(i, blocks, first=False):
@@ -257,32 +265,31 @@
     def blocks_of(steps):
         return [ring_block(way, step + 1) for step in steps for way in range(2)]
 
-    late = half_ring - LATE
     for step in range(half_ring):
-        for k in range(6):
+        for k in range(5):
             for way in range(2):
                 if active(way, step, k):
                     ring(way, step, k, 1).wait_recv()
                     if active(way, step + 1, k):
                         ring(way, step + 1, k, 0).start()
-                    if k >= 3:
+                    if k < 2:
                         pair_copy(way, step, k, odd).start()
-            if k >= n_fs:
-                continue
-            if step > late:
-                project(k, blocks_of((step - 1,)))
-        if step == late - 2:
+        if step == half_ring // 2:
             token_gather.neighbours()
-        if step == late - 1:
+        if step == half_ring - 2:
             token_gather.opposite()
-        if step == late:
-            together(t_recv.at[0, 4], n_fs * token_size).wait_recv()
-            for i in range(n_fs):
-                project(i, [z] + blocks_of(range(late)), first=True)
-    last_block = [ring_block(0, half_ring)]
-
-    pieces = wo_recv.shape[0]
-    piece = width // pieces
+    together(pair_recv.at[0], 2 * soon * slice_size * 3 // 4).wait_recv()
+    for j in range(pieces):
+        pair_piece(j, odd).start()
+    for step in range(half_ring):
+        for way in range(2):
+            if active(way, step, 4):
+                pair_copy(way, step, 4, odd).start()
+    together(t_recv.at[0, 4], n_fs * token_size).wait_recv()
+    for i in range(n_fs):
+        project(i, [z] + blocks_of(range(soon)), first=True)
+    together(pair_recv.at[1], (n_sp - 1 - 2 * soon) * slice_size * 3 // 4).wait_recv()
+    last_blocks = blocks_of(range(soon, half_ring - 1)) + [ring_block(0, half_ring)]
 
     def w_out_ref(core, j):
         def ref(i, first, length):
@@ -304,7 +311,7 @@
         return wide * scale * gain
 
     for i in range(n_fs):
-        project(i, last_block)
+        project(i, last_blocks)
         both = partial[0, i]
         query = (unit(both[:, :HD], q_gain_ref[:, lanes_x]) * HALF**-0.5).astype(BF16)
         key = unit(both[:, HD:], k_gain_ref[:, lanes_x]).astype(BF16)
@@ -350,10 +357,10 @@
     def _():
         heads[z] = qkv[z // 2]
 
-    together(pair_recv.at[0], (n_sp - 1) * slice_size).wait_recv()
-    together(pair_recv.at[1], (n_sp - 1) * slice_size // 4).wait_recv()
-    for gather in w_out_gathers:
+    for j, gather in enumerate(w_out_gathers):
+        together(pair_recv.at[2 + j], piece * 2 * PAIR).wait_recv()
         gather.own()
+    together(pair_recv.at[6], (n_sp - 1) * slice_size // 4).wait_recv()
 
     @pl.loop(0, n_fs)
     def _(i):
@@ -567,8 +574,8 @@
 
     together(send.at[0], 12 * shard_size).wait_send()
     together(send.at[1], 7 * token_size).wait_send()
-    together(send.at[2], (n_sp - 1) * slice_size * 11 // 4).wait_send()
-    together(send.at[3], (n_sp - 1) * slice_size * 5 // 4).wait_send()
+    together(send.at[2], (n_sp - 1) * slice_size * 2).wait_send()
+    together(send.at[3], (2 * n_sp - 1) * slice_size).wait_send()
     together(send.at[4], last * block * 6 * HD).wait_send()
     together(send.at[5], 7 * width * 2 * PAIR).wait_send()
     together(send.at[6], len(conv_to) * conv_size).wait_send()
@@ -627,8 +634,8 @@
             dma((10,)),
             dma((4,)),
             dma((1, 5)),
-            dma((2, half_ring, 6)),
-            dma((2,)),
+            dma((2, half_ring, 5)),
+            dma((7,)),
             pltpu.SemaphoreType.REGULAR,
             dma((n_seq,)),
             dma((1,)),

time: 124 us -> 122 us (0.984)
  Pallas kernels: 123 us -> 120 us
    pallas_call x1, Pallas kernels: 123 us -> 120 us  [on_device(): call(*[pltpu.with_memory_space_constraint(a, pltpu.HBM) for a in ins])]
where the time goes in v6:
time: 122 us; the launch traced here: 121 us
  Pallas kernels  120 us (98%)
    pallas_call x1, Pallas kernels, on_device(): call(*[pltpu.with_memory_space_constraint(a, pltpu.HBM) for a in ins])  120 us

profile of v6, /device:TPU:33, one launch (start us, length us, event | category | flops | bytes accessed | tf_op | source)
XLA Modules:
  0.0 121.2 jit_solution(2643493626759541655)
XLA Ops:
  0.0 120.4 %shard_map.145 = bf16[2,64,2048]{2,1,0:T(8,128)(2,1)S(1)} custom-call(bf16[2,64,2048]{2,1,0:T(8,128)(2,1)} %refs_0_.1, f32[1,2048]{1,0:T(1,128)} %bitcast.9, bf16[32,512]{1,0:T(8,128)(2,1)} %refs_2_.1, bf16[32,512]{1,0:T(8,128)(2,1)} %refs_3_.1, bf16[32,512]{1,0:T(8,128)(2,1)} %refs_4_.1, f32[1,512]{1,0:T(1,128)} %bitcast.10, f32[1,512]{1,0:T(1,128)} %bitcast.11, ...), custom_call_target="tpu_custom_call" | custom-call | tf_op jit(solution)/shard_map/pallas_call | solution.py:653
  120.5 0.8 copy.17

commit v7 on v6

--- a/solution.py
+++ b/solution.py
@@ -49,6 +49,7 @@
     ring_recv,
     pair_recv,
     ready,
+    pace,
     a_recv,
     kv_recv,
     o_recv,
@@ -266,6 +267,12 @@
         return [ring_block(way, step + 1) for step in steps for way in range(2)]
 
     for step in range(half_ring):
+        if step >= 2:
+
+            @pl.when(c == 1)
+            def _():
+                pl.semaphore_wait(pace, 1)
+
         for k in range(5):
             for way in range(2):
                 if active(way, step, k):
@@ -274,6 +281,12 @@
                         ring(way, step + 1, k, 0).start()
                     if k < 2:
                         pair_copy(way, step, k, odd).start()
+        if step < half_ring - 2:
+
+            @pl.when(c == 0)
+            def _():
+                pl.semaphore_signal(pace, inc=1, device_id=dict(tp=other), device_id_type=MESH)
+
         if step == half_ring // 2:
             token_gather.neighbours()
         if step == half_ring - 2:
@@ -637,6 +650,7 @@
             dma((2, half_ring, 5)),
             dma((7,)),
             pltpu.SemaphoreType.REGULAR,
+            pltpu.SemaphoreType.REGULAR,
             dma((n_seq,)),
             dma((1,)),
             dma((n_fs,)),

time: 122 us -> 122 us (level)
  no operation moved by 1% of the time
where the time goes in v7:
time: 122 us; the launch traced here: 121 us
  Pallas kernels  120 us (98%)
    pallas_call x1, Pallas kernels, on_device(): call(*[pltpu.with_memory_space_constraint(a, pltpu.HBM) for a in ins])  120 us

profile of v7, /device:TPU:33, one launch (start us, length us, event | category | flops | bytes accessed | tf_op | source)
XLA Modules:
  0.0 120.9 jit_solution(11812498654625506586)
XLA Ops:
  0.0 120.1 %shard_map.145 = bf16[2,64,2048]{2,1,0:T(8,128)(2,1)S(1)} custom-call(bf16[2,64,2048]{2,1,0:T(8,128)(2,1)} %refs_0_.1, f32[1,2048]{1,0:T(1,128)} %bitcast.9, bf16[32,512]{1,0:T(8,128)(2,1)} %refs_2_.1, bf16[32,512]{1,0:T(8,128)(2,1)} %refs_3_.1, bf16[32,512]{1,0:T(8,128)(2,1)} %refs_4_.1, f32[1,512]{1,0:T(1,128)} %bitcast.10, f32[1,512]{1,0:T(1,128)} %bitcast.11, ...), custom_call_target="tpu_custom_call" | custom-call | tf_op jit(solution)/shard_map/pallas_call | solution.py:667
  120.1 0.8 copy.17
